TPU v7x, 128 devices: a whole 4x4x4 slice. The times are simulated.
128 devices in a mesh: fs: 16 (over z, y), tp: 8 (over x, core).
Axes of the slice: x: 4, y: 4, z: 4, core: 2. Of those that a mesh axis runs over, the one named last changes fastest.
Arguments:
- query_latent_rows: bfloat16 [24576, 1024], P('fs'), may hold values from -6 to 6
- grad_q: bfloat16 [24576, 3072], P('fs', 'tp'), may hold values from -6 to 6
- head_out: bfloat16 [24576, 2048], P('fs', 'tp'), may hold values from -6 to 6
- grad_out: bfloat16 [24576, 4096], P('fs'), may hold values from -6 to 6
- proj_q: bfloat16 [1024, 256], P('fs'), may hold values from -0.5 to 0.5
- proj_o: bfloat16 [4096, 256], P('fs'), may hold values from -0.5 to 0.5
- query_up_weight: float32 [1024, 3072], P('fs', 'tp'), may hold values from -0.1875 to 0.1875
- weight_o: float32 [4096, 2048], P('fs', 'tp'), may hold values from -0.125 to 0.125
- first_q: float32 [256, 3072], P('fs', 'tp'), may hold values from -6 to 6
- second_q: float32 [256, 3072], P('fs', 'tp'), may hold values from 0.25 to 4
- first_o: float32 [256, 2048], P('fs', 'tp'), may hold values from -6 to 6
- second_o: float32 [256, 2048], P('fs', 'tp'), may hold values from 0.25 to 4
Outputs:
- new_weight_q: float32 [1024, 3072], P('fs', 'tp')
- new_weight_o: float32 [4096, 2048], P('fs', 'tp')
- new_first_q: float32 [256, 3072], P('fs', 'tp')
- new_second_q: float32 [256, 3072], P('fs', 'tp')
- new_first_o: float32 [256, 2048], P('fs', 'tp')
- new_second_o: float32 [256, 2048], P('fs', 'tp')
- step_q: float32 [1024, 3072], P('fs', 'tp')
- step_o: float32 [4096, 2048], P('fs', 'tp')
- copy_q: bfloat16 [1024, 3072], P(None, 'tp')
- copy_o: bfloat16 [4096, 2048], P(None, 'tp')
All inputs are finite; a program needn't handle non-finite values.
Results may differ from a plain program's by a relative error of at most 0.008.
Values may be sent and summed in bfloat16 or wider, within the bound.
A program may use at most 128 MiB of HBM per device.

v0:
```python
import math

import jax
import jax.numpy as jnp
from jax import lax
from jax.sharding import Mesh
from jax.sharding import PartitionSpec as P

FS = ("fs_0", "fs_1")
FS_TP = ("fs_0", "fs_1", "tp_0", "tp_1")
TP = ("tp_0", "tp_1")


beta_first = 0.8
beta_second = 0.9
epsilon = 1e-08
decay_rate = 2.0
step_rate = 0.05
contract = (((0,), (0,)), ((), ()))


def joined_along(parts, dim):
    shape = list(parts.shape[1:])
    shape[dim] *= parts.shape[0]
    return jnp.moveaxis(parts, 0, dim).reshape(shape)


def gather_packed(arrays, axis, dims):
    flat = jnp.concatenate([a.reshape(-1) for a in arrays])
    lines, at, finished = (lax.all_gather(flat, axis), 0, [])
    for a, dim in zip(arrays, dims):
        parts = lines[:, at : at + a.size].reshape(-1, *a.shape)
        finished.append(joined_along(parts, dim))
        at += a.size
    return tuple(finished)


def in_blocks(array, dim, size):
    before, after = (array.shape[:dim], array.shape[dim + 1 :])
    return jnp.moveaxis(array.reshape(*before, size, -1, *after), dim, 0)


def summed_on_arrival(array, axis, dim):
    parts = in_blocks(array, dim, lax.axis_size(axis))
    arrived = lax.all_to_all(parts, axis, split_axis=0, concat_axis=0, tiled=True)
    return arrived.astype(jnp.float32).sum(axis=0)


def over_axes(array, axes):
    for axis in axes:
        array = lax.psum(array, axis)
    return array


def side_by_side(arrays, axis, dim, along):
    widths = [a.shape[along] for a in arrays]
    both = jnp.concatenate(arrays, axis=along)
    out = lax.all_gather(both, axis, axis=dim, tiled=True)
    return tuple(jnp.split(out, [sum(widths[:k]) for k in range(1, len(widths))], axis=along))


def tokens_product(left, right):
    return lax.dot_general(left, right, contract, preferred_element_type=jnp.float32)


def exact_product(basis_column_count, gradient):
    return lax.dot_general(
        basis_column_count.astype(jnp.float32),
        gradient,
        contract,
        precision=lax.Precision.HIGHEST,
        preferred_element_type=jnp.float32,
    )


def moments(first, second, reduced, clip_scale):
    scaled = clip_scale * reduced
    first_new = beta_first * first + (1.0 - beta_first) * scaled
    second_new = beta_second * second + (1.0 - beta_second) * scaled * scaled
    return (first_new, second_new, first_new / (jnp.sqrt(second_new) + epsilon))


def per_device(
    query_latent_rows,
    grad_q,
    head_out,
    grad_out,
    proj_q,
    proj_o,
    query_up_weight,
    weight_o,
    first_q,
    second_q,
    first_o,
    second_o,
):
    rank_rows = first_q.shape[0]
    whole_q, whole_o = gather_packed((proj_q, proj_o), FS, (0, 0))
    partial_q = tokens_product(query_latent_rows, grad_q)
    partial_o = tokens_product(grad_out, head_out)
    low_q = summed_on_arrival(exact_product(whole_q, partial_q).astype(jnp.bfloat16), FS, 0)
    low_o = summed_on_arrival(exact_product(whole_o, partial_o).astype(jnp.bfloat16), FS, 0)
    sum_squares = over_axes(jnp.sum(low_q * low_q) + jnp.sum(low_o * low_o), FS_TP)
    entries = (
        rank_rows * lax.axis_size(FS) * (first_q.shape[1] + first_o.shape[1]) * lax.axis_size(TP)
    )
    clip_scale = jnp.minimum(1.0, math.sqrt(entries) / jnp.sqrt(sum_squares))
    first_nq, second_nq, direct_q = moments(first_q, second_q, low_q, clip_scale)
    first_no, second_no, direct_o = moments(first_o, second_o, low_o, clip_scale)
    pieces_in = side_by_side((direct_q, direct_o), FS, 0, 1)
    basis_q = proj_q.astype(jnp.float32)
    basis_o = proj_o.astype(jnp.float32)
    more_q = jnp.dot(
        basis_q, pieces_in[0], precision=lax.Precision.HIGHEST, preferred_element_type=jnp.float32
    )
    more_o = jnp.dot(
        basis_o, pieces_in[1], precision=lax.Precision.HIGHEST, preferred_element_type=jnp.float32
    )
    step_q = more_q + decay_rate * query_up_weight
    step_o = more_o + decay_rate * weight_o
    new_weight_q = query_up_weight - step_rate * step_q
    new_weight_o = weight_o - step_rate * step_o
    copy_q, copy_o = (
        lax.all_gather(new_weight_q.astype(jnp.bfloat16), FS, axis=0, tiled=True),
        lax.all_gather(new_weight_o.astype(jnp.bfloat16), FS, axis=0, tiled=True),
    )
    return (
        new_weight_q,
        new_weight_o,
        first_nq,
        second_nq,
        first_no,
        second_no,
        step_q,
        step_o,
        copy_q,
        copy_o,
    )


def solution(mesh):
    finer = Mesh(mesh.devices.reshape(4, 4, 4, 2), ("fs_0", "fs_1", "tp_0", "tp_1"))
    return jax.shard_map(
        per_device,
        mesh=finer,
        in_specs=(
            P(FS, None),
            P(FS, TP),
            P(FS, TP),
            P(FS, None),
            P(FS, None),
            P(FS, None),
            P(FS, TP),
            P(FS, TP),
            P(FS, TP),
            P(FS, TP),
            P(FS, TP),
            P(FS, TP),
        ),
        out_specs=(
            P(FS, TP),
            P(FS, TP),
            P(FS, TP),
            P(FS, TP),
            P(FS, TP),
            P(FS, TP),
            P(FS, TP),
            P(FS, TP),
            P(None, TP),
            P(None, TP),
        ),
        check_vma=False,
    )
```

profile of v0, /device:TPU:1, one launch (start us, length us, event | category | flops | bytes accessed | tf_op | source)
XLA Modules:
  0.0 225.4 jit_solution(798599784227551670)
XLA Ops:
  7.2 0.9 copy.32
  8.2 1.0 copy.33
  9.9 4.3 %fusion.10 = f32[1024,384]{1,0:T(8,128)} fusion(bf16[1536,1024]{1,0:T(8,128)(2,1)S(1)} %copy-done, bf16[1536,384]{1,0:T(8,128)(2,1)} %param.13), kind=kOutput, calls=%fused_computation.26 | convolution fusion | flops 1207959552 | bytes 5898240 | tf_op jit(solution)/shard_map/dot_general | solution.py:63
  14.3 10.2 %fusion.11 = f32[4096,256]{1,0:T(8,128)} fusion(bf16[1536,4096]{1,0:T(8,128)(2,1)} %param.15, bf16[1536,256]{1,0:T(8,128)(2,1)S(1)} %copy-done.5), kind=kOutput, calls=%fused_computation.27 | convolution fusion | flops 3221225472 | bytes 17563648 | tf_op jit(solution)/shard_map/dot_general | solution.py:63
  24.5 34.8 %all-gather.6.cloned.1.call-done = bf16[1310720]{0:T(1024)(128)(2,1)} async-done(((bf16[81920]{0:T(1024)(128)(2,1)}), bf16[1310720]{0:T(1024)(128)(2,1)}) %all-gather.6.cloned.1.call-update) | async-done | bytes 2621456 | tf_op jit(solution)/shard_map/all_gather | solution.py:30
  59.3 3.6 %reshape.36 = bf16[16,81920]{1,0:T(8,128)(2,1)} reshape(bf16[1310720]{0:T(1024)(128)(2,1)} %all-gather.6.cloned.1.call-done) | data formatting | bytes 5242880 | tf_op jit(solution)/shard_map/all_gather | solution.py:30
  62.8 1.9 slice.8
  64.7 3.0 %slice.9 = bf16[16,65536]{1,0:T(8,128)(2,1)} slice(bf16[16,81920]{1,0:T(8,128)(2,1)} %reshape.36), slice={[0:16], [16384:81920]} | slice | bytes 4194304 | tf_op jit(solution)/shard_map/slice | solution.py:32
  67.7 3.2 %reshape_reshape.7 = bf16[4096,256]{1,0:T(8,128)(2,1)} reshape(bf16[16,65536]{1,0:T(8,128)(2,1)} %slice.9) | data formatting | bytes 4194304 | tf_op jit(solution)/shard_map/reshape;reshape | solution.py:25
  71.0 2.1 reshape_reshape.6
  73.0 6.3 %convolution_convert_fusion.1 = bf16[256,256]{1,0:T(8,128)(2,1)} fusion(bf16[4096,256]{1,0:T(8,128)(2,1)} %reshape_reshape.7, f32[4096,256]{1,0:T(8,128)} %fusion.11), kind=kOutput, calls=%fused_computation.3 | convolution fusion | flops 3221291008 | bytes 6422528 | tf_op jit(solution)/shard_map/dot_general | solution.py:67
  79.4 4.1 %all-to-all-start.1 = ((bf16[16,16,256]{2,1,0:T(8,128)(2,1)}), bf16[16,16,256]{2,1,0:T(8,128)(2,1)S(1)}, u32[]{:S(2)}, u32[]{:S(2)}) async-start(bf16[16,16,256]{2,1,0:T(8,128)(2,1)} %bitcast.1), calls=%async_computation.1 | async-start | bytes 262144 | tf_op jit(solution)/shard_map/all_to_all | solution.py:45
  83.5 3.4 %convolution_convert_fusion = bf16[256,384]{1,0:T(8,128)(2,1)} fusion(bf16[1024,256]{1,0:T(8,128)(2,1)} %reshape_reshape.6, f32[1024,384]{1,0:T(8,128)} %fusion.10), kind=kOutput, calls=%fused_computation | convolution fusion | flops 1208057856 | bytes 2293760 | tf_op jit(solution)/shard_map/dot_general | solution.py:67
  86.9 3.4 %all-to-all-done.1 = bf16[16,16,256]{2,1,0:T(8,128)(2,1)S(1)} async-done(((bf16[16,16,256]{2,1,0:T(8,128)(2,1)}), bf16[16,16,256]{2,1,0:T(8,128)(2,1)S(1)}, u32[]{:S(2)}, u32[]{:S(2)}) %all-to-all-start.1) | async-done | bytes 131104 | tf_op jit(solution)/shard_map/all_to_all | solution.py:45
  91.0 3.5 %all-to-all-start = ((bf16[16,16,384]{2,1,0:T(8,128)(2,1)}), bf16[16,16,384]{2,1,0:T(8,128)(2,1)S(1)}, u32[]{:S(2)}, u32[]{:S(2)}) async-start(bf16[16,16,384]{2,1,0:T(8,128)(2,1)} %bitcast), calls=%async_computation | async-start | bytes 393216 | tf_op jit(solution)/shard_map/all_to_all | solution.py:45
  96.1 5.6 %all-to-all-done = bf16[16,16,384]{2,1,0:T(8,128)(2,1)S(1)} async-done(((bf16[16,16,384]{2,1,0:T(8,128)(2,1)}), bf16[16,16,384]{2,1,0:T(8,128)(2,1)S(1)}, u32[]{:S(2)}, u32[]{:S(2)}) %all-to-all-start) | async-done | bytes 196640 | tf_op jit(solution)/shard_map/all_to_all | solution.py:45
  103.6 7.0 %psum.28 = f32[]{:T(128)} all-reduce(f32[]{:T(128)S(6)} %add.41), channel_id=1, replica_groups=mesh['fs_0'=4,'fs_1'=4,'tp_0'=4,'tp_1'=2] {'fs_0'}, use_global_device_ids=true, to_apply=%region_4.0 | all-reduce | flops 1 | bytes 8 | tf_op jit(solution)/shard_map/psum | solution.py:51
  110.6 7.6 %psum.29 = f32[]{:T(128)} all-reduce(f32[]{:T(128)} %psum.28), channel_id=1, replica_groups=mesh['fs_0'=4,'fs_1'=4,'tp_0'=4,'tp_1'=2] {'fs_1'}, use_global_device_ids=true, to_apply=%region_5.0 | all-reduce | flops 1 | bytes 8 | tf_op jit(solution)/shard_map/psum | solution.py:51
  118.2 9.0 %psum.30 = f32[]{:T(128)} all-reduce(f32[]{:T(128)} %psum.29), channel_id=1, replica_groups=mesh['fs_0'=4,'fs_1'=4,'tp_0'=4,'tp_1'=2] {'tp_0'}, use_global_device_ids=true, to_apply=%region_6.0 | all-reduce | flops 1 | bytes 8 | tf_op jit(solution)/shard_map/psum | solution.py:51
  127.2 1.1 copy.28
  128.3 13.4 %psum.31 = f32[]{:T(128)} all-reduce(f32[]{:T(128)} %psum.30), channel_id=1, replica_groups=mesh['fs_0'=4,'fs_1'=4,'tp_0'=4,'tp_1'=2] {'tp_1'}, use_global_device_ids=true, to_apply=%region_7.0 | all-reduce | flops 1 | bytes 8 | tf_op jit(solution)/shard_map/psum | solution.py:51
  142.4 1.4 add_divide_fusion.1
  143.8 1.4 add_divide_fusion
  145.2 16.9 %all_gather.17 = f32[256,640]{1,0:T(8,128)S(1)} all-gather(f32[16,640]{1,0:T(8,128)S(1)} %pad_maximum_fusion.1), channel_id=1, replica_groups=mesh['fs_0'=4,'fs_1'=4,'tp_0'=4,'tp_1'=2] {'fs_0','fs_1'}, dimensions={0}, use_global_device_ids=true | all-gather | bytes 696320 | tf_op jit(solution)/shard_map/all_gather | solution.py:58
  162.9 1.2 fusion.6
  164.1 1.8 copy.29
  165.9 1.8 copy.30
  167.7 2.0 fusion.7
  169.7 20.5 %all_gather.18 = bf16[1024,384]{1,0:T(8,128)(2,1)} all-gather(bf16[64,384]{1,0:T(8,128)(2,1)S(1)} %get-tuple-element.32), channel_id=1, replica_groups=mesh['fs_0'=4,'fs_1'=4,'tp_0'=4,'tp_1'=2] {'fs_0','fs_1'}, dimensions={0}, use_global_device_ids=true | all-gather | bytes 835584 | tf_op jit(solution)/shard_map/all_gather | solution.py:124
  190.2 22.2 %all-gather.4.cloned.1.call-done = bf16[4096,256]{0,1:T(8,128)(2,1)} async-done(((bf16[256,256]{0,1:T(8,128)(2,1)}), bf16[4096,256]{0,1:T(8,128)(2,1)}) %all-gather.4.cloned.1.call-update) | async-done | bytes 2097168 | tf_op jit(solution)/shard_map/all_gather | solution.py:125
  212.4 4.1 %copy.31 = bf16[4096,256]{1,0:T(8,128)(2,1)} copy(bf16[4096,256]{0,1:T(8,128)(2,1)} %all-gather.4.cloned.1.call-done) | data formatting | bytes 4194304
  216.4 2.1 copy.35
  (22 shorter events, 4.5 us)
Async XLA Ops:
  7.2 2.7 %copy-start = (bf16[1536,1024]{1,0:T(8,128)(2,1)S(1)}, bf16[1536,1024]{1,0:T(8,128)(2,1)}, u32[]{:S(2)}) copy-start(bf16[1536,1024]{1,0:T(8,128)(2,1)} %param.12) | copy-start | bytes 9437188
  7.2 52.1 %all-gather.6.cloned.1.call-start = ((), (), s32[]{:S(2)}) async-start(), calls=%async_computation.3 | async-start | bytes 2785280 | tf_op jit(solution)/shard_map/all_gather | solution.py:30
  9.9 4.4 %copy-start.5 = (bf16[1536,256]{1,0:T(8,128)(2,1)S(1)}, bf16[1536,256]{1,0:T(8,128)(2,1)}, u32[]{:S(2)}) copy-start(bf16[1536,256]{1,0:T(8,128)(2,1)} %param.14) | copy-start | bytes 2359300
  79.4 10.9 %all-to-all-start.1 = ((bf16[16,16,256]{2,1,0:T(8,128)(2,1)}), bf16[16,16,256]{2,1,0:T(8,128)(2,1)S(1)}, u32[]{:S(2)}, u32[]{:S(2)}) async-start(bf16[16,16,256]{2,1,0:T(8,128)(2,1)} %bitcast.1), calls=%async_computation.1 | async-start | bytes 262144 | tf_op jit(solution)/shard_map/all_to_all | solution.py:45
  83.5 79.4 %copy-start.2 = (bf16[256,256]{1,0:T(8,128)(2,1)S(1)}, bf16[256,256]{1,0:T(8,128)(2,1)}, u32[]{:S(2)}) copy-start(bf16[256,256]{1,0:T(8,128)(2,1)} %param.17) | copy-start | bytes 393220
  90.3 0.7 copy-start.3
  91.0 10.7 %all-to-all-start = ((bf16[16,16,384]{2,1,0:T(8,128)(2,1)}), bf16[16,16,384]{2,1,0:T(8,128)(2,1)S(1)}, u32[]{:S(2)}, u32[]{:S(2)}) async-start(bf16[16,16,384]{2,1,0:T(8,128)(2,1)} %bitcast), calls=%async_computation | async-start | bytes 393216 | tf_op jit(solution)/shard_map/all_to_all | solution.py:45
  94.5 117.9 %all-gather.4.cloned.1.call-start = ((), (), s32[]{:S(2)}) async-start(), calls=%async_computation.2 | async-start | bytes 2228224 | tf_op jit(solution)/shard_map/all_gather | solution.py:125
  101.7 16.5 %copy-start.4 = (f32[16,384]{1,0:T(8,128)}, f32[16,384]{1,0:T(8,128)S(1)}, u32[]{:S(2)}) copy-start(f32[16,384]{1,0:T(8,128)S(1)} %convert_reduce_fusion) | copy-start | bytes 73732
  162.1 0.8 copy-start.1
Sparse Core Ops, SparseCore 0:
  10.7 48.4 all-gather.5
  164.2 48.0 all-gather.3
where the time goes:
time: 227 us; the launch traced here: 225 us
  blocking collectives  74.5 us (33%)
  waiting for transfers between devices  66 us (29%)
  local copies, waits for them, and re-layouts  28 us (12%)
  matrix products  27.5 us (12%)
  between operations  16.1 us (7%)
  starting transfers between devices  7.69 us (3%)
  other arithmetic  5.61 us (2%)
    psum x4, blocking collectives, over_axes(): array = lax.psum(array, axis)  37.1 us
    all_gather x1, waiting for transfers between devices, gather_packed(): lines, at, finished = (lax.all_gather(flat, axis), 0, [])  34.8 us
    all_gather x1, waiting for transfers between devices, per_device(): lax.all_gather(new_weight_o.astype(jnp.bfloat16), FS, axis=0, tiled=True)  22.2 us
    all_gather x1, blocking collectives, per_device(): lax.all_gather(new_weight_q.astype(jnp.bfloat16), FS, axis=0, tiled=True)  20.5 us
    all_gather x1, blocking collectives, side_by_side(): out = lax.all_gather(both, axis, axis=dim, tiled=True)  16.9 us
    dot_general x2, matrix products, tokens_product(): lax.dot_general(left, right, contract, preferred_element_type=jnp.float32)  14.5 us
    unnamed x19, local copies, waits for them, and re-layouts  14.3 us
    dot_general x2, matrix products, exact_product(): lax.dot_general(basis_column_count.astype(jnp.float32), gradient, contrac...  9.72 us
  transfers between devices with their start and end apart: 4, of which 4 were waited for; matrix products, arithmetic and copies ran while one was open for 11% of the time, Pallas kernels for 0%

commit v1 on v0

v1 whole, which is shorter than its diff:
```python
import math

import jax
import jax.numpy as jnp
from jax import lax
from jax.experimental import pallas as pl
from jax.experimental.pallas import tpu as pltpu
from jax.sharding import PartitionSpec as P

FS, TP = "fs", "tp"
SIDE = 4
N_FS, N_TP = 16, 8

beta_first = 0.8
beta_second = 0.9
epsilon = 1e-08
decay_rate = 2.0
step_rate = 0.05

BF16, F32 = jnp.bfloat16, jnp.float32


def dot(a, b):
    return lax.dot_general(a, b, (((1,), (0,)), ((), ())), preferred_element_type=F32)


def dot_t(a, b):
    return lax.dot_general(a, b, (((0,), (0,)), ((), ())), preferred_element_type=F32)


class PlaneGather:
    def __init__(self, ref_of, rows, ssem, rsem, a, b, fs_of):
        self.ref_of, self.rows, self.ss, self.rs = ref_of, rows, ssem, rsem
        self.a, self.b, self.fs_of = a, b, fs_of
        self.am = [a, (a + 3) % SIDE, (a + 1) % SIDE, (a + 2) % SIDE]
        self.bp, self.bm, self.b2 = (b + 1) % SIDE, (b + 3) % SIDE, (b + 2) % SIDE
        self.sent = []

    def part(self, half):
        h = self.rows // 2
        return {None: (0, self.rows), 0: (0, h), 1: (h, h)}[half]

    def copy(self, j, block, half, to):
        lo, n = self.part(half)
        ref = self.ref_of(block, lo, n)
        return pltpu.make_async_remote_copy(
            src_ref=ref, dst_ref=ref, send_sem=self.ss.at[j], recv_sem=self.rs.at[j],
            device_id={FS: to}, device_id_type=pl.DeviceIdType.MESH)

    def send(self, j, block, half, to):
        c = self.copy(j, block, half, to)
        c.start()
        self.sent.append(c)

    def got(self, j, block, half):
        self.copy(j, block, half, block).wait_recv()

    def along_b(self, m):
        blk = self.fs_of(self.am[m], self.b)
        self.send(4 + 2 * m, blk, None, self.fs_of(self.a, self.bp))
        self.send(5 + 2 * m, blk, None, self.fs_of(self.a, self.bm))

    def start(self):
        own = self.fs_of(self.a, self.b)
        self.send(0, own, None, self.fs_of(self.am[2], self.b))
        self.send(1, own, None, self.fs_of(self.am[1], self.b))
        self.along_b(0)
        return own

    def take_a(self, m):
        blk = self.fs_of(self.am[m], self.b)
        self.got(m - 1, blk, None)
        self.send(m + 1, blk, m - 1, self.fs_of(self.am[3 - m], self.b))
        self.along_b(m)
        return blk

    def take_a2(self):
        blk = self.fs_of(self.am[3], self.b)
        self.got(2, blk, 0)
        self.got(3, blk, 1)
        self.along_b(3)
        return blk

    def take_b(self, m):
        lo = self.fs_of(self.am[m], self.bm)
        self.got(4 + 2 * m, lo, None)
        self.send(12 + 2 * m, lo, 0, self.fs_of(self.a, self.bp))
        hi = self.fs_of(self.am[m], self.bp)
        self.got(5 + 2 * m, hi, None)
        self.send(13 + 2 * m, hi, 1, self.fs_of(self.a, self.bm))
        return lo, hi

    def take_b2(self, m):
        blk = self.fs_of(self.am[m], self.b2)
        self.got(12 + 2 * m, blk, 0)
        self.got(13 + 2 * m, blk, 1)
        return blk

    def finish(self):
        for c in self.sent:
            c.wait_send()


def moments(first, second, reduced, clip_scale):
    scaled = clip_scale * reduced
    first_new = beta_first * first + (1.0 - beta_first) * scaled
    second_new = beta_second * second + (1.0 - beta_second) * scaled * scaled
    return first_new, second_new, first_new / (jnp.sqrt(second_new) + epsilon)


def exchange_kernel(target, xq_h, gq_h, ho_h, go_h, pq_h, po_h, wq_h, wo_h, fq_h, sq_h, fo_h, so_h,
                    pf, pw, dirs, low, scale,
                    xq, gq, ho, go, wq, wo, fq, sq, fo, so, zq, zo, rs_out, rs_in, sum_tp, sum_fs,
                    in_sem, p_ss, p_rs, w_ss, w_rs, sib_ss, sib_rs, rs_ss, rs_rs, st_ss, st_rs, sf_ss, sf_rs,
                    ag_ss, ag_rs):
    i, t = lax.axis_index(FS), lax.axis_index(TP)
    z, y, c = i // SIDE, i % SIDE, t % 2
    a, b = y * (1 - c) + z * c, z * (1 - c) + y * c

    def fs_of(a_, b_):
        return a_ * (1 + 3 * c) + b_ * (4 - 3 * c)

    nq, no = pq_h.shape[0], po_h.shape[0]
    own_p = pf.at[i]
    loads = []

    def load(src, dst):
        cp = pltpu.make_async_copy(src, dst, in_sem.at[len(loads)])
        cp.start()
        loads.append(cp)
        return cp

    half = (nq + no) // 2
    p1 = load(pq_h, pf.at[i, 0, pl.ds(0, nq)])
    p2 = load(po_h.at[pl.ds(0, half - nq)], pf.at[i, 0, pl.ds(nq, half - nq)])
    p3 = load(po_h.at[pl.ds(half - nq, half)], pf.at[i, 1])
    w1, w2 = load(wq_h, wq), load(wo_h, wo)
    big = [load(go_h, go), load(xq_h, xq), load(gq_h, gq), load(ho_h, ho)]
    small = [load(s, d) for s, d in ((fq_h, fq), (sq_h, sq), (fo_h, fo), (so_h, so))]

    barrier = pltpu.get_barrier_semaphore()
    nbrs = [{FS: fs_of((a + 1) % SIDE, b)}, {FS: fs_of((a + 3) % SIDE, b)},
            {FS: fs_of(a, (b + 1) % SIDE)}, {FS: fs_of(a, (b + 3) % SIDE)}]
    nbrs += [{TP: (t + d) % N_TP} for d in range(1, N_TP)]
    for n in nbrs:
        pl.semaphore_signal(barrier, inc=1, device_id=n, device_id_type=pl.DeviceIdType.MESH)
    p1.wait()
    p2.wait()
    p3.wait()
    pl.semaphore_wait(barrier, len(nbrs))

    pg = PlaneGather(lambda blk, lo, n: pf.at[blk, c, pl.ds(lo, n)], half, p_ss, p_rs, a, b, fs_of)
    sib = {TP: t + 1 - 2 * c}
    sib_sent = []

    def sib_copy(blk, which):
        ref = pf.at[blk, which]
        return pltpu.make_async_remote_copy(
            src_ref=ref, dst_ref=ref, send_sem=sib_ss.at[blk], recv_sem=sib_rs.at[blk],
            device_id=sib, device_id_type=pl.DeviceIdType.MESH)

    def to_sib(blk):
        cp = sib_copy(blk, c)
        cp.start()
        sib_sent.append(cp)

    pg.start()

    w1.wait()
    w2.wait()
    row = 0
    for src in (wq, wo):
        for col in range(0, src.shape[1], 128):
            pw[i, row:row + src.shape[0], :] = src[:, col:col + 128].astype(BF16)
            row += src.shape[0]

    to_sib(pg.take_a(1))
    to_sib(pg.take_a(2))
    for blk in pg.take_b(0):
        to_sib(blk)
    to_sib(pg.take_a2())
    for m in (1, 2, 3):
        for blk in pg.take_b(m):
            to_sib(blk)
    for m in range(4):
        to_sib(pg.take_b2(m))

    def wait_sib(k, _):
        blk = (i + k) % N_FS
        sib_copy(blk, 1 - c).wait_recv()
        return 0

    lax.fori_loop(1, N_FS, wait_sib, 0)
    for cp in big:
        cp.wait()

    tile = 256

    def project(m, _):
        rows = pl.ds(m * tile, tile)
        whole = pf[...].reshape(N_FS, 2 * half, pf.shape[3])
        zo[rows, :] = dot(go[rows, :], whole[:, nq:, :].reshape(N_FS * no, -1)).astype(BF16)
        zq[rows, :] = dot(xq[rows, :], whole[:, :nq, :].reshape(N_FS * nq, -1)).astype(BF16)
        return 0

    lax.fori_loop(0, xq.shape[0] // tile, project, 0)
    part = jnp.concatenate([dot_t(zq[...], gq[...]), dot_t(zo[...], ho[...])], axis=1)
    rs_out[...] = part.astype(BF16).reshape(rs_out.shape)

    def rs_copy(d):
        return pltpu.make_async_remote_copy(
            src_ref=rs_out.at[(i + d) % N_FS], dst_ref=rs_in.at[d], send_sem=rs_ss.at[d], recv_sem=rs_rs,
            device_id={FS: (i + d) % N_FS}, device_id_type=pl.DeviceIdType.MESH)

    def start(make):
        def body(d, _):
            make(d).start()
            return 0
        return body

    def wait_send(make):
        def body(d, _):
            make(d).wait_send()
            return 0
        return body

    lax.fori_loop(1, N_FS, start(rs_copy), 0)

    wg = PlaneGather(lambda blk, lo, n: pw.at[blk, pl.ds(lo, n)], pw.shape[1], w_ss, w_rs, a, b, fs_of)
    wg.start()

    arrived = rs_in.at[pl.ds(1, N_FS - 1)]
    pltpu.make_async_copy(arrived, arrived, rs_rs).wait()
    reduced = rs_out[i].astype(F32)
    for d in range(1, N_FS):
        reduced = reduced + rs_in[d].astype(F32)
    low[...] = reduced
    local = jnp.sum(jnp.sum(reduced * reduced, axis=1, keepdims=True), axis=0, keepdims=True)
    sum_tp[0] = jnp.broadcast_to(local, sum_tp.shape[1:])

    def st_copy(d):
        return pltpu.make_async_remote_copy(
            src_ref=sum_tp.at[0], dst_ref=sum_tp.at[d], send_sem=st_ss.at[d], recv_sem=st_rs,
            device_id={TP: (t + d) % N_TP}, device_id_type=pl.DeviceIdType.MESH)

    lax.fori_loop(1, N_TP, start(st_copy), 0)
    wg.take_a(1)
    wg.take_a(2)
    rest = sum_tp.at[pl.ds(1, N_TP - 1)]
    pltpu.make_async_copy(rest, rest, st_rs).wait()
    sum_fs[0] = jnp.sum(sum_tp[...], axis=0)

    def sf_copy(d):
        return pltpu.make_async_remote_copy(
            src_ref=sum_fs.at[0], dst_ref=sum_fs.at[d], send_sem=sf_ss.at[d], recv_sem=sf_rs,
            device_id={FS: (i + d) % N_FS}, device_id_type=pl.DeviceIdType.MESH)

    lax.fori_loop(1, N_FS, start(sf_copy), 0)
    wg.take_b(0)
    wg.take_a2()
    rest = sum_fs.at[pl.ds(1, N_FS - 1)]
    pltpu.make_async_copy(rest, rest, sf_rs).wait()
    total = jnp.sum(sum_fs[...], axis=0)
    clip = jnp.minimum(1.0, target / jnp.sqrt(total))
    scale[...] = clip
    for cp in small:
        cp.wait()
    s = clip[0:1, 0:1]
    cq = fq.shape[1]
    _, _, dq = moments(fq[...], sq[...], low[:, :cq], s)
    _, _, do = moments(fo[...], so[...], low[:, cq:], s)
    dirs[i] = jnp.concatenate([dq, do], axis=1).astype(BF16)

    def ag_copy(d):
        return pltpu.make_async_remote_copy(
            src_ref=dirs.at[i], dst_ref=dirs.at[i], send_sem=ag_ss.at[d], recv_sem=ag_rs.at[d],
            device_id={FS: (i + d) % N_FS}, device_id_type=pl.DeviceIdType.MESH)

    lax.fori_loop(1, N_FS, start(ag_copy), 0)
    for m in (1, 2, 3):
        wg.take_b(m)
    for m in range(4):
        wg.take_b2(m)

    def ag_wait(d, _):
        blk = (i - d + N_FS) % N_FS
        pltpu.make_async_remote_copy(
            src_ref=dirs.at[blk], dst_ref=dirs.at[blk], send_sem=ag_ss.at[d], recv_sem=ag_rs.at[d],
            device_id={FS: blk}, device_id_type=pl.DeviceIdType.MESH).wait_recv()
        return 0

    lax.fori_loop(1, N_FS, ag_wait, 0)
    pg.finish()
    wg.finish()
    for cp in sib_sent:
        cp.wait_send()
    lax.fori_loop(1, N_FS, wait_send(rs_copy), 0)
    lax.fori_loop(1, N_TP, wait_send(st_copy), 0)
    lax.fori_loop(1, N_FS, wait_send(sf_copy), 0)
    lax.fori_loop(1, N_FS, wait_send(ag_copy), 0)


def update_kernel(pf, pw, dirs, low, scale, pq, po, wq, wo, fq, sq, fo, so,
                  nwq, nwo, nfq, nsq, nfo, nso, stq, sto, cpq, cpo):
    cq, co = fq.shape[1], fo.shape[1]
    nq, no = pq.shape[0], po.shape[0]
    d = dirs[...].reshape(-1, cq + co)
    dq, do = d[:, :cq], d[:, cq:]
    n = pf.shape[0]
    whole = pf[...].reshape(n, nq + no, pf.shape[3])
    mq = dot(whole[:, :nq, :].reshape(n * nq, -1), dq)
    mo = dot(whole[:, nq:, :].reshape(n * no, -1), do)
    keep = 1.0 - step_rate * decay_rate
    for col in range(0, cq, 128):
        w = pw[:, (col // 128) * nq:(col // 128 + 1) * nq, :].astype(F32).reshape(n * nq, 128)
        cpq[:, col:col + 128] = (keep * w - step_rate * mq[:, col:col + 128]).astype(BF16)
    base = (cq // 128) * nq
    for col in range(0, co, 128):
        at = base + (col // 128) * no
        w = pw[:, at:at + no, :].astype(F32).reshape(n * no, 128)
        cpo[:, col:col + 128] = (keep * w - step_rate * mo[:, col:col + 128]).astype(BF16)

    @pl.when(pl.program_id(0) == 0)
    def _():
        s = scale[0:1, 0:1]
        f, v, _ = moments(fq[...], sq[...], low[:, :cq], s)
        nfq[...] = f
        nsq[...] = v
        f, v, _ = moments(fo[...], so[...], low[:, cq:], s)
        nfo[...] = f
        nso[...] = v
        for p_, d_, w_, st_, nw_ in ((pq, dq, wq, stq, nwq), (po, do, wo, sto, nwo)):
            step = dot(p_[...], d_) + decay_rate * w_[...]
            st_[...] = step
            nw_[...] = w_[...] - step_rate * step


def per_device(query_latent_rows, grad_q, head_out, grad_out, proj_q, proj_o, query_up_weight, weight_o,
               first_q, second_q, first_o, second_o):
    nq, no, rank = proj_q.shape[0], proj_o.shape[0], proj_q.shape[1]
    cq, co = first_q.shape[1], first_o.shape[1]
    rows = first_q.shape[0]
    target = math.sqrt(rows * N_FS * (cq + co) * N_TP)
    half = (nq + no) // 2
    wrows = (nq * cq + no * co) // 128
    sds = jax.ShapeDtypeStruct
    any_ = pl.BlockSpec(memory_space=pl.ANY)
    vmem = pl.BlockSpec(memory_space=pltpu.VMEM)
    dma = pltpu.SemaphoreType.DMA
    V = pltpu.VMEM
    ins = (query_latent_rows, grad_q, head_out, grad_out, proj_q, proj_o, query_up_weight, weight_o,
           first_q, second_q, first_o, second_o)
    like = lambda x: V(x.shape, x.dtype)
    tokens = query_latent_rows.shape[0]

    def ex(*refs):
        exchange_kernel(target, *refs)

    pf, pw, dirs, low, scale = pl.pallas_call(
        ex,
        out_shape=[sds((N_FS, 2, half, rank), BF16), sds((N_FS, wrows, 128), BF16),
                   sds((N_FS, rows, cq + co), BF16), sds((rows, cq + co), F32), sds((8, 128), F32)],
        in_specs=[any_] * len(ins),
        out_specs=[vmem] * 5,
        scratch_shapes=[
            like(query_latent_rows), like(grad_q), like(head_out), like(grad_out),
            like(query_up_weight), like(weight_o), like(first_q), like(second_q), like(first_o), like(second_o),
            V((tokens, rank), BF16), V((tokens, rank), BF16),
            V((N_FS, rows, cq + co), BF16), V((N_FS, rows, cq + co), BF16),
            V((N_TP, 8, 128), F32), V((N_FS, 8, 128), F32),
            dma((13,)), dma((20,)), dma((20,)), dma((20,)), dma((20,)), dma((N_FS,)), dma((N_FS,)),
            dma((N_FS,)), dma, dma((N_TP,)), dma, dma((N_FS,)), dma, dma((N_FS,)), dma((N_FS,)),
        ],
        compiler_params=pltpu.CompilerParams(collective_id=0, has_side_effects=True,
                                             vmem_limit_bytes=48 * 1024 * 1024),
        name="exchange",
    )(*ins)

    G = 4
    n = N_FS // G
    full = lambda x: pl.BlockSpec(x.shape, lambda g: (0,) * len(x.shape))
    outs = [sds((nq, cq), F32), sds((no, co), F32), sds((rows, cq), F32), sds((rows, cq), F32),
            sds((rows, co), F32), sds((rows, co), F32), sds((nq, cq), F32), sds((no, co), F32)]
    tail = (proj_q, proj_o, query_up_weight, weight_o, first_q, second_q, first_o, second_o)
    return tuple(pl.pallas_call(
        update_kernel,
        grid=(G,),
        in_specs=[pl.BlockSpec((n, 2, half, rank), lambda g: (g, 0, 0, 0)),
                  pl.BlockSpec((n, wrows, 128), lambda g: (g, 0, 0)),
                  full(dirs), full(low), full(scale)] + [full(x) for x in tail],
        out_specs=[full(o) for o in outs] + [pl.BlockSpec((n * nq, cq), lambda g: (g, 0)),
                                             pl.BlockSpec((n * no, co), lambda g: (g, 0))],
        out_shape=outs + [sds((N_FS * nq, cq), BF16), sds((N_FS * no, co), BF16)],
        compiler_params=pltpu.CompilerParams(vmem_limit_bytes=24 * 1024 * 1024),
        name="update",
    )(pf, pw, dirs, low, scale, *tail))


def solution(mesh):
    rows, both, cols = P(FS, None), P(FS, TP), P(None, TP)
    return jax.shard_map(
        per_device,
        mesh=mesh,
        in_specs=(rows, both, both, rows, rows, rows) + (both,) * 6,
        out_specs=(both,) * 8 + (cols, cols),
        check_vma=False,
    )
```

time: 227 us -> 76.1 us (0.34)
  blocking collectives: 74.5 us -> 0 us
  waiting for transfers between devices: 66 us -> 0 us
  Pallas kernels: 0 us -> 64.2 us
  matrix products: 27.5 us -> 0 us
  local copies, waits for them, and re-layouts: 28 us -> 10.6 us
  between operations: 16.1 us -> 0.68 us
  starting transfers between devices: 7.69 us -> 0 us
  other arithmetic: 5.61 us -> 0 us
    pallas_call x0 -> x2, Pallas kernels: none -> 64.2 us  [the longest x1 60.7 us: per_device(): pl.pallas_call(ex, out_shape=[sds((N_FS, 2, half, rank), BF16), sds((N_FS...]
    all_gather x2 -> x0, waiting for transfers between devices: 57 us -> none  [the longest x1 34.8 us: gather_packed(): lines, at, finished = (lax.all_gather(flat, axis), 0, [])]
    all_gather x2 -> x0, blocking collectives: 37.4 us -> none  [the longest x1 20.5 us: per_device(): lax.all_gather(new_weight_q.astype(jnp.bfloat16), FS, axis=0, tiled=True)]
    psum x4 -> x0, blocking collectives: 37.1 us -> none  [over_axes(): array = lax.psum(array, axis)]
    dot_general x6 -> x0, matrix products: 27.5 us -> none  [the longest x2 14.5 us: tokens_product(): lax.dot_general(left, right, contract, preferred_element_type=jnp.float32)]
    all_to_all x2 -> x0, waiting for transfers between devices: 9 us -> none  [summed_on_arrival(): lax.all_to_all(parts, axis, split_axis=0, concat_axis=0, tiled=True)]
    all_to_all x2 -> x0, starting transfers between devices: 7.61 us -> none  [summed_on_arrival(): lax.all_to_all(parts, axis, split_axis=0, concat_axis=0, tiled=True)]
    another operation x2 -> x0, local copies, waits for them, and re-layouts: 5.28 us -> none  [joined_along(): return jnp.moveaxis(parts, 0, dim).reshape(shape)]
  transfers between devices with their start and end apart: 4 -> 0, of which waited for: 4 -> 0; matrix products, arithmetic and copies ran while one was open for 11% -> 0% of each run, Pallas kernels for 0% -> 0%
where the time goes in v1:
time: 76.1 us; the launch traced here: 75.5 us
  Pallas kernels  64.2 us (84%)
  local copies, waits for them, and re-layouts  10.6 us (14%)
    pallas_call x1, Pallas kernels, per_device(): pl.pallas_call(ex, out_shape=[sds((N_FS, 2, half, rank), BF16), sds((N_FS...  60.7 us
    unnamed x22, local copies, waits for them, and re-layouts  10.6 us
    pallas_call x1, Pallas kernels, per_device(): pl.pallas_call(update_kernel, grid=(G,), in_specs=[pl.BlockSpec((n, 2, ha...  3.49 us

profile of v1, /device:TPU:1, one launch (start us, length us, event | category | flops | bytes accessed | tf_op | source)
XLA Modules:
  0.0 75.5 jit_solution(11611358557349462190)
XLA Ops:
  0.6 0.0 copy-start.1
  0.7 1.3 %copy-done.1 = bf16[1536,384]{1,0:T(8,128)(2,1)S(1)} copy-done((bf16[1536,384]{1,0:T(8,128)(2,1)S(1)}, bf16[1536,384]{1,0:T(8,128)(2,1)}, u32[]{:S(2)}) %copy-start.1) | copy-done | bytes 1179672
  1.9 0.0 copy-start.2
  1.9 0.9 %copy-done.2 = f32[256,256]{1,0:T(8,128)S(1)} copy-done((f32[256,256]{1,0:T(8,128)S(1)}, f32[256,256]{1,0:T(8,128)}, u32[]{:S(2)}) %copy-start.2) | copy-done | bytes 262168
  2.9 0.0 copy-start.3
  2.9 1.1 %copy-done.3 = bf16[1536,256]{1,0:T(8,128)(2,1)S(1)} copy-done((bf16[1536,256]{1,0:T(8,128)(2,1)S(1)}, bf16[1536,256]{1,0:T(8,128)(2,1)}, u32[]{:S(2)}) %copy-start.3) | copy-done | bytes 786456
  4.0 0.0 copy-start.4
  4.0 0.9 %copy-done.4 = bf16[256,256]{1,0:T(8,128)(2,1)S(1)} copy-done((bf16[256,256]{1,0:T(8,128)(2,1)S(1)}, bf16[256,256]{1,0:T(8,128)(2,1)}, u32[]{:S(2)}) %copy-start.4) | copy-done | bytes 131096
  4.9 0.0 copy-start.5
  4.9 0.9 %copy-done.5 = f32[64,384]{1,0:T(8,128)S(1)} copy-done((f32[64,384]{1,0:T(8,128)S(1)}, f32[64,384]{1,0:T(8,128)}, u32[]{:S(2)}) %copy-start.5) | copy-done | bytes 98328
  5.8 0.0 copy-start.6
  5.8 0.8 %copy-done.6 = bf16[64,256]{1,0:T(8,128)(2,1)S(1)} copy-done((bf16[64,256]{1,0:T(8,128)(2,1)S(1)}, bf16[64,256]{1,0:T(8,128)(2,1)}, u32[]{:S(2)}) %copy-start.6) | copy-done | bytes 32792
  6.6 0.0 copy-start.7
  6.6 0.7 copy-done.7
  7.3 0.0 copy-start.8
  7.3 0.7 copy-done.8
  8.0 0.0 copy-start.9
  8.0 0.7 copy-done.9
  8.8 0.0 copy-start.10
  8.8 0.7 copy-done.10
  9.5 60.7 %exchange.1 = (bf16[16,2,160,256]{3,2,1,0:T(8,128)(2,1)S(1)}, bf16[16,704,128]{2,1,0:T(8,128)(2,1)}, bf16[16,16,640]{2,1,0:T(8,128)(2,1)S(1)}, f32[16,640]{1,0:T(8,128)S(1)}, f32[8,128]{1,0:T(8,128)S(1)}) custom-call(bf16[1536,1024]{1,0:T(8,128)(2,1)} %refs_0_.1, bf16[1536,384]{1,0:T(8,128)(2,1)S(1)} %copy-done.1, bf16[1536,256]{1,0:T(8,128)(2,1)S(1)} %copy-done.3, ...), custom_call_target="tpu_custom_call" | custom-call | tf_op jit(solution)/shard_map/exchange/pallas_call | solution.py:359
  70.2 0.0 copy-start
  70.2 1.8 %copy-done = bf16[16,704,128]{2,1,0:T(8,128)(2,1)S(1)} copy-done((bf16[16,704,128]{2,1,0:T(8,128)(2,1)S(1)}, bf16[16,704,128]{2,1,0:T(8,128)(2,1)}, u32[]{:S(2)}) %copy-start) | copy-done | bytes 2883608
  72.0 3.5 %update.1 = (f32[64,384]{1,0:T(8,128)}, f32[256,256]{1,0:T(8,128)}, f32[16,384]{1,0:T(8,128)}, f32[16,384]{1,0:T(8,128)}, f32[16,256]{1,0:T(8,128)}, /*index=5*/...) custom-call(bf16[16,2,160,256]{3,2,1,0:T(8,128)(2,1)S(1)} %get-tuple, ...), custom_call_target="tpu_custom_call" | custom-call | tf_op jit(solution)/shard_map/update/pallas_call | solution.py:385
Async XLA Ops:
  0.6 1.3 %copy-start.1 = (bf16[1536,384]{1,0:T(8,128)(2,1)S(1)}, bf16[1536,384]{1,0:T(8,128)(2,1)}, u32[]{:S(2)}) copy-start(bf16[1536,384]{1,0:T(8,128)(2,1)} %refs_1_.1) | copy-start | bytes 3538948
  1.9 0.9 %copy-start.2 = (f32[256,256]{1,0:T(8,128)S(1)}, f32[256,256]{1,0:T(8,128)}, u32[]{:S(2)}) copy-start(f32[256,256]{1,0:T(8,128)} %wo.1) | copy-start | bytes 786436
  2.9 1.1 %copy-start.3 = (bf16[1536,256]{1,0:T(8,128)(2,1)S(1)}, bf16[1536,256]{1,0:T(8,128)(2,1)}, u32[]{:S(2)}) copy-start(bf16[1536,256]{1,0:T(8,128)(2,1)} %refs_2_.1) | copy-start | bytes 2359300
  4.0 0.9 %copy-start.4 = (bf16[256,256]{1,0:T(8,128)(2,1)S(1)}, bf16[256,256]{1,0:T(8,128)(2,1)}, u32[]{:S(2)}) copy-start(bf16[256,256]{1,0:T(8,128)(2,1)} %po.1) | copy-start | bytes 393220
  4.9 0.9 %copy-start.5 = (f32[64,384]{1,0:T(8,128)S(1)}, f32[64,384]{1,0:T(8,128)}, u32[]{:S(2)}) copy-start(f32[64,384]{1,0:T(8,128)} %wq.1) | copy-start | bytes 294916
  5.8 0.8 %copy-start.6 = (bf16[64,256]{1,0:T(8,128)(2,1)S(1)}, bf16[64,256]{1,0:T(8,128)(2,1)}, u32[]{:S(2)}) copy-start(bf16[64,256]{1,0:T(8,128)(2,1)} %pq.1) | copy-start | bytes 98308
  6.6 0.7 copy-start.7
  7.3 0.7 copy-start.8
  8.0 0.7 copy-start.9
  8.8 0.7 copy-start.10
  70.2 1.8 %copy-start = (bf16[16,704,128]{2,1,0:T(8,128)(2,1)S(1)}, bf16[16,704,128]{2,1,0:T(8,128)(2,1)}, u32[]{:S(2)}) copy-start(bf16[16,704,128]{2,1,0:T(8,128)(2,1)} %get-tuple-element.16.pw) | copy-start | bytes 8650756

commit v2 on v1

v2 whole, which is shorter than its diff:
```python
import math

import jax
import jax.numpy as jnp
from jax import lax
from jax.experimental import pallas as pl
from jax.experimental.pallas import tpu as pltpu
from jax.sharding import PartitionSpec as P

FS, TP = "fs", "tp"
SIDE = 4
N_FS, N_TP = 16, 8

beta_first = 0.8
beta_second = 0.9
epsilon = 1e-08
decay_rate = 2.0
step_rate = 0.05

BF16, F32 = jnp.bfloat16, jnp.float32

NP, NW = 2, 3
PLAN = {
    "0": [(0, 0)],
    "1": [(1, 0)],
    "2": [(0, 1), (2, 0)],
    "3": [(0, 2), (1, 1)],
    "4": [(0, 3), (0, 4), (1, 2), (2, 1)],
    "5": [(0, 5), (1, 3), (1, 4), (2, 2)],
    "6": [(1, 5), (2, 3), (2, 4)],
    "7": [(2, 5)],
}


def dot(a, b):
    return lax.dot_general(a, b, (((1,), (0,)), ((), ())), preferred_element_type=F32)


def dot_t(a, b):
    return lax.dot_general(a, b, (((0,), (0,)), ((), ())), preferred_element_type=F32)


class PlaneGather:
    def __init__(self, ref_of, rows, ssem, rsem, a, b, fs_of, direct=False):
        self.direct = direct
        self.ref_of, self.rows, self.ss, self.rs = ref_of, rows, ssem, rsem
        self.a, self.b, self.fs_of = a, b, fs_of
        self.am = [a, (a + 3) % SIDE, (a + 1) % SIDE, (a + 2) % SIDE]
        self.bp, self.bm, self.b2 = (b + 1) % SIDE, (b + 3) % SIDE, (b + 2) % SIDE
        self.sent = []

    def part(self, half):
        h = self.rows // 2
        return {None: (0, self.rows), 0: (0, h), 1: (h, h)}[half]

    def copy(self, j, block, half, to):
        lo, n = self.part(half)
        ref = self.ref_of(block, lo, n)
        return pltpu.make_async_remote_copy(
            src_ref=ref, dst_ref=ref, send_sem=self.ss.at[j], recv_sem=self.rs.at[j],
            device_id={FS: to}, device_id_type=pl.DeviceIdType.MESH)

    def send(self, j, block, half, to):
        c = self.copy(j, block, half, to)
        c.start()
        self.sent.append(c)

    def got(self, j, block, half):
        self.copy(j, block, half, block).wait_recv()

    def along_b(self, m):
        blk = self.fs_of(self.am[m], self.b)
        self.send(4 + 2 * m, blk, None, self.fs_of(self.a, self.bp))
        self.send(5 + 2 * m, blk, None, self.fs_of(self.a, self.bm))

    def start(self):
        own = self.fs_of(self.a, self.b)
        self.send(0, own, None, self.fs_of(self.am[2], self.b))
        self.send(1, own, None, self.fs_of(self.am[1], self.b))
        if self.direct:
            self.send(2, own, None, self.fs_of(self.am[3], self.b))
        self.along_b(0)
        return own

    def take_a(self, m):
        blk = self.fs_of(self.am[m], self.b)
        self.got(m - 1, blk, None)
        if not self.direct:
            self.send(m + 1, blk, m - 1, self.fs_of(self.am[3 - m], self.b))
        self.along_b(m)
        return blk

    def take_a2(self):
        blk = self.fs_of(self.am[3], self.b)
        if self.direct:
            self.got(2, blk, None)
        else:
            self.got(2, blk, 0)
            self.got(3, blk, 1)
        self.along_b(3)
        return blk

    def take_b(self, m):
        lo = self.fs_of(self.am[m], self.bm)
        self.got(4 + 2 * m, lo, None)
        self.send(12 + 2 * m, lo, 0, self.fs_of(self.a, self.bp))
        hi = self.fs_of(self.am[m], self.bp)
        self.got(5 + 2 * m, hi, None)
        self.send(13 + 2 * m, hi, 1, self.fs_of(self.a, self.bm))
        return lo, hi

    def take_b2(self, m):
        blk = self.fs_of(self.am[m], self.b2)
        self.got(12 + 2 * m, blk, 0)
        self.got(13 + 2 * m, blk, 1)
        return blk

    def finish(self):
        for c in self.sent:
            c.wait_send()


def moments(first, second, reduced, clip_scale):
    scaled = clip_scale * reduced
    first_new = beta_first * first + (1.0 - beta_first) * scaled
    second_new = beta_second * second + (1.0 - beta_second) * scaled * scaled
    return first_new, second_new, first_new / (jnp.sqrt(second_new) + epsilon)


def exchange_kernel(target, xq_h, gq_h, ho_h, go_h, pq_h, po_h, wq_h, wo_h, fq_h, sq_h, fo_h, so_h,
                    pf, pw, lowg, low, scale,
                    xq, gq, ho, go, wq, wo, fq, sq, fo, so, ho_t, gq_t, grad_o, grad_q, acc, rs_out, rs_in,
                    sum_tp, sum_fs,
                    in_sem, p_ss, p_rs, w_ss, w_rs, sib_ss, sib_rs, rs_ss, rs_rs,
                    st_ss, st_rs, sf_ss, sf_rs, ag_ss, ag_rs):
    i, t = lax.axis_index(FS), lax.axis_index(TP)
    z, y, c = i // SIDE, i % SIDE, t % 2
    a, b = y * (1 - c) + z * c, z * (1 - c) + y * c

    def fs_of(a_, b_):
        return a_ * (1 + 3 * c) + b_ * (4 - 3 * c)

    nq, no = pq_h.shape[0], po_h.shape[0]
    loads = []

    def load(src, dst):
        cp = pltpu.make_async_copy(src, dst, in_sem.at[len(loads)])
        cp.start()
        loads.append(cp)
        return cp

    half = (nq + no) // 2
    p1 = load(pq_h, pf.at[i, 0, pl.ds(0, nq)])
    p2 = load(po_h.at[pl.ds(0, half - nq)], pf.at[i, 0, pl.ds(nq, half - nq)])
    p3 = load(po_h.at[pl.ds(half - nq, half)], pf.at[i, 1])
    own_f32 = [load(s, d) for s, d in ((wq_h, wq), (wo_h, wo), (fq_h, fq), (fo_h, fo), (sq_h, sq), (so_h, so))]
    l_ho, l_gq = load(ho_h, ho), load(gq_h, gq)
    step = go.shape[1] // 4
    l_go = [load(go_h.at[:, pl.ds(k * step, step)], go.at[:, pl.ds(k * step, step)]) for k in range(4)]
    l_xq = load(xq_h, xq)

    barrier = pltpu.get_barrier_semaphore()
    nbrs = [{FS: fs_of((a + d) % SIDE, b)} for d in (1, 2, 3)] + [
        {FS: fs_of(a, (b + d) % SIDE)} for d in (1, 2, 3)]
    nbrs += [{TP: (t + d) % N_TP} for d in range(1, N_TP)]
    for n in nbrs:
        pl.semaphore_signal(barrier, inc=1, device_id=n, device_id_type=pl.DeviceIdType.MESH)
    for cp in (p1, p2, p3):
        cp.wait()
    pl.semaphore_wait(barrier, len(nbrs))

    piece = half // NP
    pgs = [PlaneGather(lambda blk, lo, n, g=g: pf.at[blk, c, pl.ds(g * piece + lo, n)], piece,
                       p_ss.at[g], p_rs.at[g], a, b, fs_of, direct=True) for g in range(NP)]
    wpiece = pw.shape[1] // NW
    wgs = [PlaneGather(lambda blk, lo, n, g=g: pw.at[blk, pl.ds(g * wpiece + lo, n)], wpiece,
                       w_ss.at[g], w_rs.at[g], a, b, fs_of) for g in range(NW)]
    sib = {TP: t + 1 - 2 * c}
    sib_sent = []

    def sib_copy(g, blk, which):
        ref = pf.at[blk, which, pl.ds(g * piece, piece)]
        return pltpu.make_async_remote_copy(
            src_ref=ref, dst_ref=ref, send_sem=sib_ss.at[g, blk], recv_sem=sib_rs.at[g, blk],
            device_id=sib, device_id_type=pl.DeviceIdType.MESH)

    def to_sib(g, *blks):
        for blk in blks:
            cp = sib_copy(g, blk, c)
            cp.start()
            sib_sent.append(cp)

    for g in pgs:
        g.start()

    for cp in own_f32:
        cp.wait()
    row = 0
    for src in (wq, wo, fq, fo, sq, so):
        for col in range(0, src.shape[1], 128):
            part = src[:, col:col + 128]
            if src is wq or src is wo:
                part = part * (1.0 - step_rate * decay_rate)
            pw[i, row:row + src.shape[0], :] = part.astype(BF16)
            row += src.shape[0]

    def w_stage(w, s):
        g = wgs[w]
        if s == 0:
            g.start()
        elif s == 1:
            g.take_a(1)
            g.take_a(2)
        elif s == 2:
            g.take_b(0)
            g.take_a2()
        elif s == 3:
            g.take_b(1)
            g.take_b(2)
        elif s == 4:
            g.take_b(3)
        else:
            for m in range(4):
                g.take_b2(m)

    def fill(slot):
        for w, s in PLAN.get(slot, ()):
            w_stage(w, s)

    def gradient_o(k):
        l_go[k].wait()
        for at in range(k * step, (k + 1) * step, 256):
            grad_o[:, at:at + 256] = dot(ho_t[...], go[:, at:at + 256]).astype(BF16)

    def gradient_q(k):
        for at in range(k * 512, (k + 1) * 512, 256):
            grad_q[:, at:at + 256] = dot(gq_t[...], xq[:, at:at + 256]).astype(BF16)

    def wait_sib(*blks):
        for blk in blks:
            for g in range(NP):
                sib_copy(g, blk, 1 - c).wait_recv()

    def project_o(*blks):
        out = None
        for blk in blks:
            p = pf[blk].reshape(2 * half, -1)[nq:]
            d = dot(grad_o[:, pl.ds(pl.multiple_of(blk * no, no), no)], p)
            out = d if out is None else out + d
        return out

    a1, a2, a3 = (a + 3) % SIDE, (a + 1) % SIDE, (a + 2) % SIDE
    b1, b2, b3 = (b + 3) % SIDE, (b + 1) % SIDE, (b + 2) % SIDE
    fill("0")
    l_ho.wait()
    ho_t[...] = ho[...].T
    for g, pg in enumerate(pgs):
        to_sib(g, pg.take_a(1))
        to_sib(g, pg.take_a(2))
    fill("1")
    l_gq.wait()
    gq_t[...] = gq[...].T
    gradient_o(0)
    for g, pg in enumerate(pgs):
        to_sib(g, *pg.take_b(0))
        to_sib(g, pg.take_a2())
    fill("2")
    gradient_o(1)
    for g, pg in enumerate(pgs):
        to_sib(g, *pg.take_b(1))
        to_sib(g, *pg.take_b(2))
    fill("3")
    gradient_o(2)
    for g, pg in enumerate(pgs):
        to_sib(g, *pg.take_b(3))
    fill("4")
    gradient_o(3)
    for g, pg in enumerate(pgs):
        to_sib(g, pg.take_b2(0))
    l_xq.wait()
    gradient_q(0)
    for g, pg in enumerate(pgs):
        to_sib(g, pg.take_b2(1))
        to_sib(g, pg.take_b2(2))
    gradient_q(1)
    near = [fs_of(p, q) for p in (a1, a2) for q in (b1, b2)] + [fs_of(a, b1), fs_of(a, b2), fs_of(a1, b), fs_of(a2, b)]
    wait_sib(*near)
    acc[...] = project_o(i, *near)
    for g, pg in enumerate(pgs):
        to_sib(g, pg.take_b2(3))
    fill("5")
    far = [fs_of(a3, b), fs_of(a, b3), fs_of(a3, b1), fs_of(a3, b2), fs_of(a1, b3), fs_of(a2, b3), fs_of(a3, b3)]
    wait_sib(*far)
    part_o = acc[...] + project_o(*far)
    part_q = dot(grad_q[...], pf[:, 0, 0:nq, :].reshape(N_FS * nq, -1))
    cq = fq.shape[1]
    rs_out[:, :, cq:] = part_o.T.astype(BF16).reshape(N_FS, -1, part_o.shape[0])
    rs_out[:, :, :cq] = part_q.T.astype(BF16).reshape(N_FS, -1, part_q.shape[0])

    def rs_copy(d):
        return pltpu.make_async_remote_copy(
            src_ref=rs_out.at[(i + d) % N_FS], dst_ref=rs_in.at[d], send_sem=rs_ss.at[d], recv_sem=rs_rs,
            device_id={FS: (i + d) % N_FS}, device_id_type=pl.DeviceIdType.MESH)

    def start(make):
        def body(d, _):
            make(d).start()
            return 0
        return body

    def wait_send(make):
        def body(d, _):
            make(d).wait_send()
            return 0
        return body

    lax.fori_loop(1, N_FS, start(rs_copy), 0)
    fill("6")
    arrived = rs_in.at[pl.ds(1, N_FS - 1)]
    pltpu.make_async_copy(arrived, arrived, rs_rs).wait()
    reduced = rs_out[i].astype(F32)
    for d in range(1, N_FS):
        reduced = reduced + rs_in[d].astype(F32)
    low[...] = reduced
    lowg[i] = reduced.astype(BF16)
    sum_tp[t] = jnp.full(sum_tp.shape[1:], jnp.sum(reduced * reduced), F32)

    def st_copy(d, src=None):
        return pltpu.make_async_remote_copy(
            src_ref=sum_tp.at[t], dst_ref=sum_tp.at[t], send_sem=st_ss.at[d], recv_sem=st_rs.at[d],
            device_id={TP: (t + d) % N_TP}, device_id_type=pl.DeviceIdType.MESH)

    def sf_copy(d):
        return pltpu.make_async_remote_copy(
            src_ref=sum_fs.at[i], dst_ref=sum_fs.at[i], send_sem=sf_ss.at[d], recv_sem=sf_rs.at[d],
            device_id={FS: (i + d) % N_FS}, device_id_type=pl.DeviceIdType.MESH)

    def ag_copy(d):
        return pltpu.make_async_remote_copy(
            src_ref=lowg.at[i], dst_ref=lowg.at[i], send_sem=ag_ss.at[d], recv_sem=ag_rs.at[d],
            device_id={FS: (i + d) % N_FS}, device_id_type=pl.DeviceIdType.MESH)

    def arrivals(buf, me, n, axis, sems):
        def body(d, _):
            blk = (me - d + n) % n
            pltpu.make_async_remote_copy(
                src_ref=buf.at[blk], dst_ref=buf.at[blk], send_sem=sems.at[d], recv_sem=sems.at[d],
                device_id={axis: blk}, device_id_type=pl.DeviceIdType.MESH).wait_recv()
            return 0
        lax.fori_loop(1, n, body, 0)

    lax.fori_loop(1, N_TP, start(st_copy), 0)
    lax.fori_loop(1, N_FS, start(ag_copy), 0)
    fill("7")
    arrivals(sum_tp, t, N_TP, TP, st_rs)
    sum_fs[i] = jnp.sum(sum_tp[...], axis=0)
    lax.fori_loop(1, N_FS, start(sf_copy), 0)
    fill("8")
    arrivals(lowg, i, N_FS, FS, ag_rs)
    fill("9")
    arrivals(sum_fs, i, N_FS, FS, sf_rs)
    scale[...] = jnp.minimum(1.0, target / jnp.sqrt(jnp.sum(sum_fs[...], axis=0)))
    for g in pgs + wgs:
        g.finish()
    for cp in sib_sent:
        cp.wait_send()
    lax.fori_loop(1, N_FS, wait_send(rs_copy), 0)
    lax.fori_loop(1, N_TP, wait_send(st_copy), 0)
    lax.fori_loop(1, N_FS, wait_send(sf_copy), 0)
    lax.fori_loop(1, N_FS, wait_send(ag_copy), 0)


def update_kernel(pf, pw, lowg, low, scale, pq, po, wq, wo, fq, sq, fo, so,
                  nwq, nwo, nfq, nsq, nfo, nso, stq, sto, cpq, cpo, dirs):
    cq, co = fq.shape[1], fo.shape[1]
    nq, no, rows = pq.shape[0], po.shape[0], fq.shape[0]
    g = pl.program_id(0)
    n = cpq.shape[0] // nq
    blocks = (cq + co) // 128
    at_o = (cq // 128) * nq
    at_f = at_o + (co // 128) * no
    s = scale[0:1, 0:1]

    @pl.when(g == 0)
    def _():
        for j in range(blocks):
            f = pw[:, at_f + j * rows:at_f + (j + 1) * rows, :].astype(F32)
            v = pw[:, at_f + (blocks + j) * rows:at_f + (blocks + j + 1) * rows, :].astype(F32)
            l = lowg[:, :, j * 128:(j + 1) * 128].astype(F32)
            d = moments(f, v, l, s)[2]
            dirs[:, j * 128:(j + 1) * 128] = (-step_rate * d).reshape(-1, 128).astype(BF16)

    dq, do = dirs[:, :cq], dirs[:, cq:]
    own = pl.ds(g * n, n)
    whole = pf[own].reshape(n, nq + no, pf.shape[3])
    mq = dot(whole[:, :nq, :].reshape(n * nq, -1), dq)
    mo = dot(whole[:, nq:, :].reshape(n * no, -1), do)
    for col in range(0, cq, 128):
        w = pw[own, (col // 128) * nq:(col // 128 + 1) * nq, :].astype(F32).reshape(n * nq, 128)
        cpq[:, col:col + 128] = (w + mq[:, col:col + 128]).astype(BF16)
    for col in range(0, co, 128):
        at = at_o + (col // 128) * no
        w = pw[own, at:at + no, :].astype(F32).reshape(n * no, 128)
        cpo[:, col:col + 128] = (w + mo[:, col:col + 128]).astype(BF16)

    @pl.when(g == 0)
    def _():
        f, v, _ = moments(fq[...], sq[...], low[:, :cq], s)
        nfq[...] = f
        nsq[...] = v
        f, v, _ = moments(fo[...], so[...], low[:, cq:], s)
        nfo[...] = f
        nso[...] = v
        for p_, d_, w_, st_, nw_ in ((pq, dq, wq, stq, nwq), (po, do, wo, sto, nwo)):
            step = dot(p_[...], d_) * (-1.0 / step_rate) + decay_rate * w_[...]
            st_[...] = step
            nw_[...] = w_[...] - step_rate * step


def per_device(query_latent_rows, grad_q, head_out, grad_out, proj_q, proj_o, query_up_weight, weight_o,
               first_q, second_q, first_o, second_o):
    nq, no, rank = proj_q.shape[0], proj_o.shape[0], proj_q.shape[1]
    cq, co = first_q.shape[1], first_o.shape[1]
    rows = first_q.shape[0]
    target = math.sqrt(rows * N_FS * (cq + co) * N_TP)
    half = (nq + no) // 2
    wrows = (nq * cq + no * co + 2 * rows * (cq + co)) // 128
    sds = jax.ShapeDtypeStruct
    dma = pltpu.SemaphoreType.DMA
    V = pltpu.VMEM
    ins = (query_latent_rows, grad_q, head_out, grad_out, proj_q, proj_o, query_up_weight, weight_o,
           first_q, second_q, first_o, second_o)
    like = lambda x: V(x.shape, x.dtype)
    tokens = query_latent_rows.shape[0]

    def ex(*refs):
        exchange_kernel(target, *refs)

    gathered = pl.pallas_call(
        ex,
        out_shape=[V((N_FS, 2, half, rank), BF16), V((N_FS, wrows, 128), BF16),
                   V((N_FS, rows, cq + co), BF16), V((rows, cq + co), F32), V((8, 128), F32)],
        in_specs=[pl.BlockSpec(memory_space=pltpu.HBM)] * len(ins),
        out_specs=[pl.BlockSpec(memory_space=pltpu.VMEM)] * 5,
        scratch_shapes=[
            like(query_latent_rows), like(grad_q), like(head_out), like(grad_out),
            like(query_up_weight), like(weight_o), like(first_q), like(second_q), like(first_o), like(second_o),
            V((co, tokens), BF16), V((cq, tokens), BF16), V((co, N_FS * no), BF16), V((cq, N_FS * nq), BF16),
            V((co, rank), F32), V((N_FS, rows, cq + co), BF16), V((N_FS, rows, cq + co), BF16),
            V((N_TP, 8, 128), F32), V((N_FS, 8, 128), F32),
            dma((16,)), dma((NP, 20)), dma((NP, 20)), dma((NW, 20)), dma((NW, 20)),
            dma((NP, N_FS)), dma((NP, N_FS)),
            dma((N_FS,)), dma, dma((N_TP,)), dma((N_TP,)),
            dma((N_FS,)), dma((N_FS,)), dma((N_FS,)), dma((N_FS,)),
        ],
        compiler_params=pltpu.CompilerParams(collective_id=0, has_side_effects=True,
                                             vmem_limit_bytes=48 * 1024 * 1024),
        name="exchange",
    )(*[pltpu.with_memory_space_constraint(x, pltpu.HBM) for x in ins])

    G = 4
    n = N_FS // G
    full = lambda x: pl.BlockSpec(x.shape, lambda g: (0,) * len(x.shape))
    outs = [sds((nq, cq), F32), sds((no, co), F32), sds((rows, cq), F32), sds((rows, cq), F32),
            sds((rows, co), F32), sds((rows, co), F32), sds((nq, cq), F32), sds((no, co), F32)]
    ops = (*gathered, proj_q, proj_o, query_up_weight, weight_o, first_q, second_q, first_o, second_o)
    return tuple(pl.pallas_call(
        update_kernel,
        grid=(G,),
        in_specs=[full(x) for x in ops],
        out_specs=[full(o) for o in outs] + [pl.BlockSpec((n * nq, cq), lambda g: (g, 0)),
                                             pl.BlockSpec((n * no, co), lambda g: (g, 0))],
        out_shape=outs + [sds((N_FS * nq, cq), BF16), sds((N_FS * no, co), BF16)],
        scratch_shapes=[V((rows * N_FS, cq + co), BF16)],
        compiler_params=pltpu.CompilerParams(vmem_limit_bytes=24 * 1024 * 1024),
        name="update",
    )(*ops))


def solution(mesh):
    rows, both, cols = P(FS, None), P(FS, TP), P(None, TP)
    return jax.shard_map(
        per_device,
        mesh=mesh,
        in_specs=(rows, both, both, rows, rows, rows) + (both,) * 6,
        out_specs=(both,) * 8 + (cols, cols),
        check_vma=False,
    )
```

time: 76.1 us -> 55.3 us (0.73)
  local copies, waits for them, and re-layouts: 10.6 us -> 0.03 us
  Pallas kernels: 64.2 us -> 53.8 us
    unnamed x22 -> x16, local copies, waits for them, and re-layouts: 10.6 us -> 0.03 us
    pallas_call x2, Pallas kernels: 64.2 us -> 53.8 us  [the longest x1 49.8 us: per_device(): pl.pallas_call(ex, out_shape=[V((N_FS, 2, half, rank), BF16), V((N_FS, wr...]
where the time goes in v2:
time: 55.3 us; the launch traced here: 54.6 us
  Pallas kernels  53.8 us (97%)
  between operations  0.78 us (1%)
    pallas_call x1, Pallas kernels, per_device(): pl.pallas_call(ex, out_shape=[V((N_FS, 2, half, rank), BF16), V((N_FS, wr...  49.8 us
    pallas_call x1, Pallas kernels, per_device(): pl.pallas_call(update_kernel, grid=(G,), in_specs=[full(x) for x in ops],...  3.94 us

profile of v2, /device:TPU:1, one launch (start us, length us, event | category | flops | bytes accessed | tf_op | source)
XLA Modules:
  0.0 54.6 jit_solution(15449149959539070748)
XLA Ops:
  0.6 0.0 copy-start.7
  0.7 0.0 copy-start.6
  0.7 0.0 copy-start.5
  0.7 0.0 copy-start.4
  0.7 0.0 copy-start
  0.7 0.0 copy-start.2
  0.7 0.0 copy-start.1
  0.7 0.0 copy-start.3
  0.7 49.8 %exchange.1 = (bf16[16,2,160,256]{3,2,1,0:T(8,128)(2,1)S(1)}, bf16[16,864,128]{2,1,0:T(8,128)(2,1)S(1)}, bf16[16,16,640]{2,1,0:T(8,128)(2,1)S(1)}, f32[16,640]{1,0:T(8,128)S(1)}, f32[8,128]{1,0:T(8,128)S(1)}) custom-call(bf16[1536,1024]{1,0:T(8,128)(2,1)} %refs_0_.1, bf16[1536,384]{1,0:T(8,128)(2,1)} %refs_1_.1, bf16[1536,256]{1,0:T(8,128)(2,1)} %refs_2_.1, ...), custom_call_target="tpu_custom_call" | custom-call | tf_op jit(solution)/shard_map/exchange/pallas_call | solution.py:439
  50.6 0.0 copy-done.7
  50.6 0.0 copy-done.6
  50.6 0.0 copy-done.5
  50.6 0.0 copy-done.4
  50.6 0.0 copy-done
  50.6 0.0 copy-done.2
  50.6 0.0 copy-done.1
  50.6 0.0 copy-done.3
  50.6 3.9 %update.1 = (f32[64,384]{1,0:T(8,128)}, f32[256,256]{1,0:T(8,128)}, f32[16,384]{1,0:T(8,128)}, f32[16,384]{1,0:T(8,128)}, f32[16,256]{1,0:T(8,128)}, /*index=5*/...) custom-call(bf16[16,2,160,256]{3,2,1,0:T(8,128)(2,1)S(1)} %get-tuple, ...), custom_call_target="tpu_custom_call" | custom-call | tf_op jit(solution)/shard_map/update/pallas_call | solution.py:467
Async XLA Ops:
  0.6 49.9 %copy-start.7 = (f32[16,256]{1,0:T(8,128)S(1)}, f32[16,256]{1,0:T(8,128)}, u32[]{:S(2)}) copy-start(f32[16,256]{1,0:T(8,128)} %so.1) | copy-start | bytes 49156
  0.7 49.9 %copy-start.6 = (f32[16,256]{1,0:T(8,128)S(1)}, f32[16,256]{1,0:T(8,128)}, u32[]{:S(2)}) copy-start(f32[16,256]{1,0:T(8,128)} %fo.1) | copy-start | bytes 49156
  0.7 49.9 %copy-start.5 = (f32[16,384]{1,0:T(8,128)S(1)}, f32[16,384]{1,0:T(8,128)}, u32[]{:S(2)}) copy-start(f32[16,384]{1,0:T(8,128)} %sq.1) | copy-start | bytes 73732
  0.7 49.9 %copy-start.4 = (f32[16,384]{1,0:T(8,128)S(1)}, f32[16,384]{1,0:T(8,128)}, u32[]{:S(2)}) copy-start(f32[16,384]{1,0:T(8,128)} %fq.1) | copy-start | bytes 73732
  0.7 49.9 %copy-start = (f32[256,256]{1,0:T(8,128)S(1)}, f32[256,256]{1,0:T(8,128)}, u32[]{:S(2)}) copy-start(f32[256,256]{1,0:T(8,128)} %wo.1) | copy-start | bytes 786436
  0.7 49.9 %copy-start.2 = (f32[64,384]{1,0:T(8,128)S(1)}, f32[64,384]{1,0:T(8,128)}, u32[]{:S(2)}) copy-start(f32[64,384]{1,0:T(8,128)} %wq.1) | copy-start | bytes 294916
  0.7 49.9 %copy-start.1 = (bf16[256,256]{1,0:T(8,128)(2,1)S(1)}, bf16[256,256]{1,0:T(8,128)(2,1)}, u32[]{:S(2)}) copy-start(bf16[256,256]{1,0:T(8,128)(2,1)} %po.1) | copy-start | bytes 393220
  0.7 49.9 %copy-start.3 = (bf16[64,256]{1,0:T(8,128)(2,1)S(1)}, bf16[64,256]{1,0:T(8,128)(2,1)}, u32[]{:S(2)}) copy-start(bf16[64,256]{1,0:T(8,128)(2,1)} %pq.1) | copy-start | bytes 98308

commit v3 on v2

--- a/solution.py
+++ b/solution.py
@@ -19,17 +19,16 @@
 
 BF16, F32 = jnp.bfloat16, jnp.float32
 
-NP, NW = 2, 3
-PLAN = {
-    "0": [(0, 0)],
-    "1": [(1, 0)],
-    "2": [(0, 1), (2, 0)],
-    "3": [(0, 2), (1, 1)],
-    "4": [(0, 3), (0, 4), (1, 2), (2, 1)],
-    "5": [(0, 5), (1, 3), (1, 4), (2, 2)],
-    "6": [(1, 5), (2, 3), (2, 4)],
-    "7": [(2, 5)],
-}
+NP, NW = 1, 1
+ORDER = [
+    ("w", 0, 0), ("t",), ("g", 0), ("g", 1), ("g", 2),
+    ("a", 1), ("a", 2), ("b", 0), ("g", 3), ("a", 3),
+    ("g", 4), ("g", 5), ("g", 6), ("g", 7), ("b", 1), ("b", 2),
+    ("g", 8), ("b", 3), ("g", 9), ("g", 10), ("g", 11),
+    ("c", 0), ("w", 0, 1), ("g", 12), ("g", 13), ("g", 14), ("g", 15), ("c", 1), ("c", 2), ("q", 0), ("q", 1),
+    ("q", 2), ("q", 3), ("near",), ("far",), ("c", 3), ("w", 0, 2), ("send",),
+    ("w", 0, 3), ("w", 0, 4), ("reduce",), ("w", 0, 5), ("clip",), ("lows",),
+]
 
 
 def dot(a, b):
@@ -129,10 +128,10 @@
 
 def exchange_kernel(target, xq_h, gq_h, ho_h, go_h, pq_h, po_h, wq_h, wo_h, fq_h, sq_h, fo_h, so_h,
                     pf, pw, lowg, low, scale,
-                    xq, gq, ho, go, wq, wo, fq, sq, fo, so, ho_t, gq_t, grad_o, grad_q, acc, rs_out, rs_in,
-                    sum_tp, sum_fs,
+                    xq, gq, ho, go, wq, wo, fq, sq, fo, so, ho_t, gq_t, grad_o, grad_q, acc, acc_q, rs_out, rs_in,
+                    sums,
                     in_sem, p_ss, p_rs, w_ss, w_rs, sib_ss, sib_rs, rs_ss, rs_rs,
-                    st_ss, st_rs, sf_ss, sf_rs, ag_ss, ag_rs):
+                    sum_ss, sum_rs, ag_ss, ag_rs):
     i, t = lax.axis_index(FS), lax.axis_index(TP)
     z, y, c = i // SIDE, i % SIDE, t % 2
     a, b = y * (1 - c) + z * c, z * (1 - c) + y * c
@@ -223,18 +222,21 @@
             for m in range(4):
                 g.take_b2(m)
 
-    def fill(slot):
-        for w, s in PLAN.get(slot, ()):
-            w_stage(w, s)
+    def transposes():
+        l_ho.wait()
+        ho_t[...] = ho[...].T
+        l_gq.wait()
+        gq_t[...] = gq[...].T
 
     def gradient_o(k):
-        l_go[k].wait()
-        for at in range(k * step, (k + 1) * step, 256):
-            grad_o[:, at:at + 256] = dot(ho_t[...], go[:, at:at + 256]).astype(BF16)
+        if k % 4 == 0:
+            l_go[k // 4].wait()
+        grad_o[:, k * 256:k * 256 + 256] = dot(ho_t[...], go[:, k * 256:k * 256 + 256]).astype(BF16)
 
     def gradient_q(k):
-        for at in range(k * 512, (k + 1) * 512, 256):
-            grad_q[:, at:at + 256] = dot(gq_t[...], xq[:, at:at + 256]).astype(BF16)
+        if k == 0:
+            l_xq.wait()
+        grad_q[:, k * 256:k * 256 + 256] = dot(gq_t[...], xq[:, k * 256:k * 256 + 256]).astype(BF16)
 
     def wait_sib(*blks):
         for blk in blks:
@@ -251,51 +253,15 @@
 
     a1, a2, a3 = (a + 3) % SIDE, (a + 1) % SIDE, (a + 2) % SIDE
     b1, b2, b3 = (b + 3) % SIDE, (b + 1) % SIDE, (b + 2) % SIDE
-    fill("0")
-    l_ho.wait()
-    ho_t[...] = ho[...].T
-    for g, pg in enumerate(pgs):
-        to_sib(g, pg.take_a(1))
-        to_sib(g, pg.take_a(2))
-    fill("1")
-    l_gq.wait()
-    gq_t[...] = gq[...].T
-    gradient_o(0)
-    for g, pg in enumerate(pgs):
-        to_sib(g, *pg.take_b(0))
-        to_sib(g, pg.take_a2())
-    fill("2")
-    gradient_o(1)
-    for g, pg in enumerate(pgs):
-        to_sib(g, *pg.take_b(1))
-        to_sib(g, *pg.take_b(2))
-    fill("3")
-    gradient_o(2)
-    for g, pg in enumerate(pgs):
-        to_sib(g, *pg.take_b(3))
-    fill("4")
-    gradient_o(3)
-    for g, pg in enumerate(pgs):
-        to_sib(g, pg.take_b2(0))
-    l_xq.wait()
-    gradient_q(0)
-    for g, pg in enumerate(pgs):
-        to_sib(g, pg.take_b2(1))
-        to_sib(g, pg.take_b2(2))
-    gradient_q(1)
     near = [fs_of(p, q) for p in (a1, a2) for q in (b1, b2)] + [fs_of(a, b1), fs_of(a, b2), fs_of(a1, b), fs_of(a2, b)]
-    wait_sib(*near)
-    acc[...] = project_o(i, *near)
-    for g, pg in enumerate(pgs):
-        to_sib(g, pg.take_b2(3))
-    fill("5")
-    far = [fs_of(a3, b), fs_of(a, b3), fs_of(a3, b1), fs_of(a3, b2), fs_of(a1, b3), fs_of(a2, b3), fs_of(a3, b3)]
-    wait_sib(*far)
-    part_o = acc[...] + project_o(*far)
-    part_q = dot(grad_q[...], pf[:, 0, 0:nq, :].reshape(N_FS * nq, -1))
+    far = [fs_of(a3, b), fs_of(a, b3), fs_of(a3, b1), fs_of(a3, b2), fs_of(a1, b3), fs_of(a2, b3)]
+    last = fs_of(a3, b3)
+
+    def project_near():
+        wait_sib(*near)
+        acc[...] = project_o(i, *near)
+
     cq = fq.shape[1]
-    rs_out[:, :, cq:] = part_o.T.astype(BF16).reshape(N_FS, -1, part_o.shape[0])
-    rs_out[:, :, :cq] = part_q.T.astype(BF16).reshape(N_FS, -1, part_q.shape[0])
 
     def rs_copy(d):
         return pltpu.make_async_remote_copy(
@@ -314,26 +280,28 @@
             return 0
         return body
 
-    lax.fori_loop(1, N_FS, start(rs_copy), 0)
-    fill("6")
-    arrived = rs_in.at[pl.ds(1, N_FS - 1)]
-    pltpu.make_async_copy(arrived, arrived, rs_rs).wait()
-    reduced = rs_out[i].astype(F32)
-    for d in range(1, N_FS):
-        reduced = reduced + rs_in[d].astype(F32)
-    low[...] = reduced
-    lowg[i] = reduced.astype(BF16)
-    sum_tp[t] = jnp.full(sum_tp.shape[1:], jnp.sum(reduced * reduced), F32)
-
-    def st_copy(d, src=None):
-        return pltpu.make_async_remote_copy(
-            src_ref=sum_tp.at[t], dst_ref=sum_tp.at[t], send_sem=st_ss.at[d], recv_sem=st_rs.at[d],
-            device_id={TP: (t + d) % N_TP}, device_id_type=pl.DeviceIdType.MESH)
-
-    def sf_copy(d):
-        return pltpu.make_async_remote_copy(
-            src_ref=sum_fs.at[i], dst_ref=sum_fs.at[i], send_sem=sf_ss.at[d], recv_sem=sf_rs.at[d],
-            device_id={FS: (i + d) % N_FS}, device_id_type=pl.DeviceIdType.MESH)
+    def project_q(*zrows):
+        out = None
+        for zr in zrows:
+            p = pf[pl.ds(zr * SIDE, SIDE), 0, 0:nq, :].reshape(SIDE * nq, -1)
+            d = dot(grad_q[:, pl.ds(pl.multiple_of(zr * SIDE * nq, SIDE * nq), SIDE * nq)], p)
+            out = d if out is None else out + d
+        return out
+
+    def project_far():
+        wait_sib(*far)
+        acc[...] += project_o(*far)
+        acc_q[...] = project_q(z, (z + 1) % SIDE, (z + 3) % SIDE)
+
+    def send_partials():
+        wait_sib(last)
+        part_o = acc[...] + project_o(last)
+        part_q = acc_q[...] + project_q((z + 2) % SIDE)
+        rs_out[:, :, cq:] = part_o.T.astype(BF16).reshape(N_FS, -1, part_o.shape[0])
+        rs_out[:, :, :cq] = part_q.T.astype(BF16).reshape(N_FS, -1, part_q.shape[0])
+        lax.fori_loop(1, N_FS, start(rs_copy), 0)
+
+    me = i * N_TP + t
 
     def ag_copy(d):
         return pltpu.make_async_remote_copy(
@@ -349,24 +317,57 @@
             return 0
         lax.fori_loop(1, n, body, 0)
 
-    lax.fori_loop(1, N_TP, start(st_copy), 0)
-    lax.fori_loop(1, N_FS, start(ag_copy), 0)
-    fill("7")
-    arrivals(sum_tp, t, N_TP, TP, st_rs)
-    sum_fs[i] = jnp.sum(sum_tp[...], axis=0)
-    lax.fori_loop(1, N_FS, start(sf_copy), 0)
-    fill("8")
-    arrivals(lowg, i, N_FS, FS, ag_rs)
-    fill("9")
-    arrivals(sum_fs, i, N_FS, FS, sf_rs)
-    scale[...] = jnp.minimum(1.0, target / jnp.sqrt(jnp.sum(sum_fs[...], axis=0)))
+    zs, ys, ts = [(z + d) % SIDE for d in range(SIDE)], [(y + d) % SIDE for d in range(SIDE)], []
+    for d in range(N_TP):
+        ts.append(((t // 2 + d // 2) % SIDE) * 2 + (c + d % 2) % 2)
+    distance = lambda d: sum(min(k, SIDE - k) for k in (d[0], d[1], d[2] // 2)) * 2 + d[2] % 2
+    far_first = sorted(((dz, dy, dt) for dz in range(SIDE) for dy in range(SIDE) for dt in range(N_TP)),
+                       key=distance, reverse=True)[:-1]
+    others = sums.at[pl.ds(0, N_FS * N_TP - 1)]
+
+    def reduce_partials():
+        arrived = rs_in.at[pl.ds(1, N_FS - 1)]
+        pltpu.make_async_copy(arrived, arrived, rs_rs).wait()
+        reduced = rs_out[i].astype(F32)
+        for d in range(1, N_FS):
+            reduced = reduced + rs_in[d].astype(F32)
+        low[...] = reduced
+        lowg[i] = reduced.astype(BF16)
+        sums[me] = jnp.full(sums.shape[1:], jnp.sum(reduced * reduced), F32)
+        for dz, dy, dt in far_first:
+            pltpu.make_async_remote_copy(
+                src_ref=sums.at[me], dst_ref=sums.at[me], send_sem=sum_ss, recv_sem=sum_rs,
+                device_id={FS: zs[dz] * SIDE + ys[dy], TP: ts[dt]}, device_id_type=pl.DeviceIdType.MESH).start()
+        lax.fori_loop(1, N_FS, start(ag_copy), 0)
+
+    def clip():
+        pltpu.make_async_copy(others, others, sum_rs).wait()
+        scale[...] = jnp.broadcast_to(
+            jnp.minimum(1.0, target / jnp.sqrt(jnp.sum(sums[...], axis=0))), scale.shape)
+
+    def from_a(m):
+        for g, pg in enumerate(pgs):
+            to_sib(g, pg.take_a(m) if m < 3 else pg.take_a2())
+
+    def from_b(m):
+        for g, pg in enumerate(pgs):
+            to_sib(g, *pg.take_b(m))
+
+    def from_b2(m):
+        for g, pg in enumerate(pgs):
+            to_sib(g, pg.take_b2(m))
+
+    steps = dict(a=from_a, b=from_b, c=from_b2, w=w_stage, t=transposes, g=gradient_o, q=gradient_q, near=project_near, far=project_far,
+                 send=send_partials, reduce=reduce_partials, clip=clip,
+                 lows=lambda: arrivals(lowg, i, N_FS, FS, ag_rs))
+    for name, *args in ORDER:
+        steps[name](*args)
+    pltpu.make_async_copy(others, others, sum_ss).wait()
     for g in pgs + wgs:
         g.finish()
     for cp in sib_sent:
         cp.wait_send()
     lax.fori_loop(1, N_FS, wait_send(rs_copy), 0)
-    lax.fori_loop(1, N_TP, wait_send(st_copy), 0)
-    lax.fori_loop(1, N_FS, wait_send(sf_copy), 0)
     lax.fori_loop(1, N_FS, wait_send(ag_copy), 0)
 
 
@@ -446,19 +447,18 @@
             like(query_latent_rows), like(grad_q), like(head_out), like(grad_out),
             like(query_up_weight), like(weight_o), like(first_q), like(second_q), like(first_o), like(second_o),
             V((co, tokens), BF16), V((cq, tokens), BF16), V((co, N_FS * no), BF16), V((cq, N_FS * nq), BF16),
-            V((co, rank), F32), V((N_FS, rows, cq + co), BF16), V((N_FS, rows, cq + co), BF16),
-            V((N_TP, 8, 128), F32), V((N_FS, 8, 128), F32),
+            V((co, rank), F32), V((cq, rank), F32), V((N_FS, rows, cq + co), BF16), V((N_FS, rows, cq + co), BF16),
+            V((N_FS * N_TP, 1, 128), F32),
             dma((16,)), dma((NP, 20)), dma((NP, 20)), dma((NW, 20)), dma((NW, 20)),
             dma((NP, N_FS)), dma((NP, N_FS)),
-            dma((N_FS,)), dma, dma((N_TP,)), dma((N_TP,)),
-            dma((N_FS,)), dma((N_FS,)), dma((N_FS,)), dma((N_FS,)),
+            dma((N_FS,)), dma, dma, dma, dma((N_FS,)), dma((N_FS,)),
         ],
         compiler_params=pltpu.CompilerParams(collective_id=0, has_side_effects=True,
                                              vmem_limit_bytes=48 * 1024 * 1024),
         name="exchange",
     )(*[pltpu.with_memory_space_constraint(x, pltpu.HBM) for x in ins])
 
-    G = 4
+    G = 2
     n = N_FS // G
     full = lambda x: pl.BlockSpec(x.shape, lambda g: (0,) * len(x.shape))
     outs = [sds((nq, cq), F32), sds((no, co), F32), sds((rows, cq), F32), sds((rows, cq), F32),

time: 55.3 us -> 50.6 us (0.915); the launches traced: 54.6 us -> 50.5 us
  Pallas kernels: 53.8 us -> 49.7 us
    pallas_call x1, Pallas kernels: 49.8 us -> 46.3 us  [per_device(): pl.pallas_call(ex, out_shape=[V((N_FS, 2, half, rank), BF16), V((N_FS, wr...]
where the time goes in v3:
time: 50.6 us; the launch traced here: 50.5 us
  Pallas kernels  49.7 us (98%)
  between operations  0.78 us (2%)
    pallas_call x1, Pallas kernels, per_device(): pl.pallas_call(ex, out_shape=[V((N_FS, 2, half, rank), BF16), V((N_FS, wr...  46.3 us
    pallas_call x1, Pallas kernels, per_device(): pl.pallas_call(update_kernel, grid=(G,), in_specs=[full(x) for x in ops],...  3.39 us

profile of v3, /device:TPU:1, one launch (start us, length us, event | category | flops | bytes accessed | tf_op | source)
XLA Modules:
  0.0 50.5 jit_solution(16566441821157813728)
XLA Ops:
  0.6 0.0 copy-start.7
  0.7 0.0 copy-start.6
  0.7 0.0 copy-start.5
  0.7 0.0 copy-start.4
  0.7 0.0 copy-start
  0.7 0.0 copy-start.2
  0.7 0.0 copy-start.1
  0.7 0.0 copy-start.3
  0.7 46.3 %exchange.1 = (bf16[16,2,160,256]{3,2,1,0:T(8,128)(2,1)S(1)}, bf16[16,864,128]{2,1,0:T(8,128)(2,1)S(1)}, bf16[16,16,640]{2,1,0:T(8,128)(2,1)S(1)}, f32[16,640]{1,0:T(8,128)S(1)}, f32[8,128]{1,0:T(8,128)S(1)}) custom-call(bf16[1536,1024]{1,0:T(8,128)(2,1)} %refs_0_.1, bf16[1536,384]{1,0:T(8,128)(2,1)} %refs_1_.1, bf16[1536,256]{1,0:T(8,128)(2,1)} %refs_2_.1, ...), custom_call_target="tpu_custom_call" | custom-call | tf_op jit(solution)/shard_map/exchange/pallas_call | solution.py:440
  47.0 0.0 copy-done.7
  47.0 0.0 copy-done.6
  47.1 0.0 copy-done.5
  47.1 0.0 copy-done.4
  47.1 0.0 copy-done
  47.1 0.0 copy-done.2
  47.1 0.0 copy-done.1
  47.1 0.0 copy-done.3
  47.1 3.4 %update.1 = (f32[64,384]{1,0:T(8,128)}, f32[256,256]{1,0:T(8,128)}, f32[16,384]{1,0:T(8,128)}, f32[16,384]{1,0:T(8,128)}, f32[16,256]{1,0:T(8,128)}, /*index=5*/...) custom-call(bf16[16,2,160,256]{3,2,1,0:T(8,128)(2,1)S(1)} %get-tuple, ...), custom_call_target="tpu_custom_call" | custom-call | tf_op jit(solution)/shard_map/update/pallas_call | solution.py:467
Async XLA Ops:
  0.6 46.4 %copy-start.7 = (f32[16,256]{1,0:T(8,128)S(1)}, f32[16,256]{1,0:T(8,128)}, u32[]{:S(2)}) copy-start(f32[16,256]{1,0:T(8,128)} %so.1) | copy-start | bytes 49156
  0.7 46.4 %copy-start.6 = (f32[16,256]{1,0:T(8,128)S(1)}, f32[16,256]{1,0:T(8,128)}, u32[]{:S(2)}) copy-start(f32[16,256]{1,0:T(8,128)} %fo.1) | copy-start | bytes 49156
  0.7 46.4 %copy-start.5 = (f32[16,384]{1,0:T(8,128)S(1)}, f32[16,384]{1,0:T(8,128)}, u32[]{:S(2)}) copy-start(f32[16,384]{1,0:T(8,128)} %sq.1) | copy-start | bytes 73732
  0.7 46.4 %copy-start.4 = (f32[16,384]{1,0:T(8,128)S(1)}, f32[16,384]{1,0:T(8,128)}, u32[]{:S(2)}) copy-start(f32[16,384]{1,0:T(8,128)} %fq.1) | copy-start | bytes 73732
  0.7 46.4 %copy-start = (f32[256,256]{1,0:T(8,128)S(1)}, f32[256,256]{1,0:T(8,128)}, u32[]{:S(2)}) copy-start(f32[256,256]{1,0:T(8,128)} %wo.1) | copy-start | bytes 786436
  0.7 46.4 %copy-start.2 = (f32[64,384]{1,0:T(8,128)S(1)}, f32[64,384]{1,0:T(8,128)}, u32[]{:S(2)}) copy-start(f32[64,384]{1,0:T(8,128)} %wq.1) | copy-start | bytes 294916
  0.7 46.4 %copy-start.1 = (bf16[256,256]{1,0:T(8,128)(2,1)S(1)}, bf16[256,256]{1,0:T(8,128)(2,1)}, u32[]{:S(2)}) copy-start(bf16[256,256]{1,0:T(8,128)(2,1)} %po.1) | copy-start | bytes 393220
  0.7 46.4 %copy-start.3 = (bf16[64,256]{1,0:T(8,128)(2,1)S(1)}, bf16[64,256]{1,0:T(8,128)(2,1)}, u32[]{:S(2)}) copy-start(bf16[64,256]{1,0:T(8,128)(2,1)} %pq.1) | copy-start | bytes 98308

commit v4 on v3

--- a/solution.py
+++ b/solution.py
@@ -19,16 +19,9 @@
 
 BF16, F32 = jnp.bfloat16, jnp.float32
 
-NP, NW = 1, 1
-ORDER = [
-    ("w", 0, 0), ("t",), ("g", 0), ("g", 1), ("g", 2),
-    ("a", 1), ("a", 2), ("b", 0), ("g", 3), ("a", 3),
-    ("g", 4), ("g", 5), ("g", 6), ("g", 7), ("b", 1), ("b", 2),
-    ("g", 8), ("b", 3), ("g", 9), ("g", 10), ("g", 11),
-    ("c", 0), ("w", 0, 1), ("g", 12), ("g", 13), ("g", 14), ("g", 15), ("c", 1), ("c", 2), ("q", 0), ("q", 1),
-    ("q", 2), ("q", 3), ("near",), ("far",), ("c", 3), ("w", 0, 2), ("send",),
-    ("w", 0, 3), ("w", 0, 4), ("reduce",), ("w", 0, 5), ("clip",), ("lows",),
-]
+CHUNKS = 4
+NW = 1
+ORDER = [('w', 0, 0), ('t',), ('g', 0), ('g', 1), ('g', 2), ('a', 1), ('a', 2), ('b', 0), ('g', 3), ('a', 3), ('g', 4), ('g', 5), ('xa', 1), ('xa', 2), ('xb', 0), ('b', 1), ('b', 2), ('g', 6), ('g', 7), ('b', 3), ('w', 0, 1), ('xa', 3), ('c', 0), ('g', 8), ('g', 9), ('xb', 1), ('xb', 2), ('c', 1), ('c', 2), ('g', 10), ('g', 11), ('xb', 3), ('c', 3), ('xc', 0), ('w', 0, 2), ('g', 12), ('g', 13), ('g', 14), ('g', 15), ('q', 0), ('q', 1), ('xc', 1), ('xc', 2), ('q', 2), ('q', 3), ('xc', 3), ('near',), ('far',), ('w', 0, 3), ('send',), ('w', 0, 4), ('reduce',), ('w', 0, 5), ('clip',), ('lows',)]
 
 
 def dot(a, b):
@@ -130,7 +123,7 @@
                     pf, pw, lowg, low, scale,
                     xq, gq, ho, go, wq, wo, fq, sq, fo, so, ho_t, gq_t, grad_o, grad_q, acc, acc_q, rs_out, rs_in,
                     sums,
-                    in_sem, p_ss, p_rs, w_ss, w_rs, sib_ss, sib_rs, rs_ss, rs_rs,
+                    in_sem, p_ss, p_rs, w_ss, w_rs, sib_ss, sib_rs, x_ss, x_rs, rs_ss, rs_rs,
                     sum_ss, sum_rs, ag_ss, ag_rs):
     i, t = lax.axis_index(FS), lax.axis_index(TP)
     z, y, c = i // SIDE, i % SIDE, t % 2
@@ -168,29 +161,44 @@
         cp.wait()
     pl.semaphore_wait(barrier, len(nbrs))
 
-    piece = half // NP
-    pgs = [PlaneGather(lambda blk, lo, n, g=g: pf.at[blk, c, pl.ds(g * piece + lo, n)], piece,
-                       p_ss.at[g], p_rs.at[g], a, b, fs_of, direct=True) for g in range(NP)]
+    quarter = half // 2
+    par = (t // 2) % 2
+    pg = PlaneGather(lambda blk, lo, n: pf.at[blk, c, pl.ds(pl.multiple_of(par * quarter, 16) + lo, n)], quarter,
+                     p_ss, p_rs, a, b, fs_of, direct=True)
     wpiece = pw.shape[1] // NW
     wgs = [PlaneGather(lambda blk, lo, n, g=g: pw.at[blk, pl.ds(g * wpiece + lo, n)], wpiece,
                        w_ss.at[g], w_rs.at[g], a, b, fs_of) for g in range(NW)]
     sib = {TP: t + 1 - 2 * c}
-    sib_sent = []
-
-    def sib_copy(g, blk, which):
-        ref = pf.at[blk, which, pl.ds(g * piece, piece)]
+    sent = []
+
+    def sib_copy(blk, which):
+        ref = pf.at[blk, which]
         return pltpu.make_async_remote_copy(
-            src_ref=ref, dst_ref=ref, send_sem=sib_ss.at[g, blk], recv_sem=sib_rs.at[g, blk],
+            src_ref=ref, dst_ref=ref, send_sem=sib_ss.at[blk], recv_sem=sib_rs.at[blk],
             device_id=sib, device_id_type=pl.DeviceIdType.MESH)
 
-    def to_sib(g, *blks):
+    def x_copy(blk, parity, side):
+        ref = pf.at[blk, c, pl.ds(pl.multiple_of(parity * quarter, 16) + side * (quarter // 2), quarter // 2)]
+        return pltpu.make_async_remote_copy(
+            src_ref=ref, dst_ref=ref, send_sem=x_ss.at[side, blk], recv_sem=x_rs.at[side, blk],
+            device_id={TP: ((t // 2 + (1, 3)[side]) % SIDE) * 2 + c}, device_id_type=pl.DeviceIdType.MESH)
+
+    def to_x(*blks):
         for blk in blks:
-            cp = sib_copy(g, blk, c)
+            for side in (0, 1):
+                cp = x_copy(blk, par, side)
+                cp.start()
+                sent.append(cp)
+
+    def from_x(*blks):
+        for blk in blks:
+            for side in (0, 1):
+                x_copy(blk, 1 - par, side).wait_recv()
+            cp = sib_copy(blk, c)
             cp.start()
-            sib_sent.append(cp)
-
-    for g in pgs:
-        g.start()
+            sent.append(cp)
+
+    pg.start()
 
     for cp in own_f32:
         cp.wait()
@@ -240,8 +248,7 @@
 
     def wait_sib(*blks):
         for blk in blks:
-            for g in range(NP):
-                sib_copy(g, blk, 1 - c).wait_recv()
+            sib_copy(blk, 1 - c).wait_recv()
 
     def project_o(*blks):
         out = None
@@ -263,22 +270,19 @@
 
     cq = fq.shape[1]
 
-    def rs_copy(d):
+    zs, ys, ts = [(z + d) % SIDE for d in range(SIDE)], [(y + d) % SIDE for d in range(SIDE)], []
+    for d in range(N_TP):
+        ts.append(((t // 2 + d // 2) % SIDE) * 2 + (c + d % 2) % 2)
+    distance = lambda d: sum(min(k, SIDE - k) for k in (d[0], d[1], d[2] // 2)) * 2 + d[2] % 2
+    far_first = sorted(((dz, dy, dt) for dz in range(SIDE) for dy in range(SIDE) for dt in range(N_TP)),
+                       key=distance, reverse=True)[:-1]
+    plane_far_first = [(dz, dy) for dz, dy, dt in far_first if dt == 0]
+
+    def rs_copy(dz, dy):
+        d, to = dz * SIDE + dy, zs[dz] * SIDE + ys[dy]
         return pltpu.make_async_remote_copy(
-            src_ref=rs_out.at[(i + d) % N_FS], dst_ref=rs_in.at[d], send_sem=rs_ss.at[d], recv_sem=rs_rs,
-            device_id={FS: (i + d) % N_FS}, device_id_type=pl.DeviceIdType.MESH)
-
-    def start(make):
-        def body(d, _):
-            make(d).start()
-            return 0
-        return body
-
-    def wait_send(make):
-        def body(d, _):
-            make(d).wait_send()
-            return 0
-        return body
+            src_ref=rs_out.at[to], dst_ref=rs_in.at[d], send_sem=rs_ss.at[d], recv_sem=rs_rs,
+            device_id={FS: to}, device_id_type=pl.DeviceIdType.MESH)
 
     def project_q(*zrows):
         out = None
@@ -299,30 +303,22 @@
         part_q = acc_q[...] + project_q((z + 2) % SIDE)
         rs_out[:, :, cq:] = part_o.T.astype(BF16).reshape(N_FS, -1, part_o.shape[0])
         rs_out[:, :, :cq] = part_q.T.astype(BF16).reshape(N_FS, -1, part_q.shape[0])
-        lax.fori_loop(1, N_FS, start(rs_copy), 0)
+        for dz, dy in plane_far_first:
+            rs_copy(dz, dy).start()
 
     me = i * N_TP + t
 
-    def ag_copy(d):
+    def ag_copy(dz, dy, back=False):
+        d, to = dz * SIDE + dy, zs[dz] * SIDE + ys[dy]
+        ref = lowg.at[zs[-dz] * SIDE + ys[-dy] if back else i]
         return pltpu.make_async_remote_copy(
-            src_ref=lowg.at[i], dst_ref=lowg.at[i], send_sem=ag_ss.at[d], recv_sem=ag_rs.at[d],
-            device_id={FS: (i + d) % N_FS}, device_id_type=pl.DeviceIdType.MESH)
-
-    def arrivals(buf, me, n, axis, sems):
-        def body(d, _):
-            blk = (me - d + n) % n
-            pltpu.make_async_remote_copy(
-                src_ref=buf.at[blk], dst_ref=buf.at[blk], send_sem=sems.at[d], recv_sem=sems.at[d],
-                device_id={axis: blk}, device_id_type=pl.DeviceIdType.MESH).wait_recv()
-            return 0
-        lax.fori_loop(1, n, body, 0)
-
-    zs, ys, ts = [(z + d) % SIDE for d in range(SIDE)], [(y + d) % SIDE for d in range(SIDE)], []
-    for d in range(N_TP):
-        ts.append(((t // 2 + d // 2) % SIDE) * 2 + (c + d % 2) % 2)
-    distance = lambda d: sum(min(k, SIDE - k) for k in (d[0], d[1], d[2] // 2)) * 2 + d[2] % 2
-    far_first = sorted(((dz, dy, dt) for dz in range(SIDE) for dy in range(SIDE) for dt in range(N_TP)),
-                       key=distance, reverse=True)[:-1]
+            src_ref=ref, dst_ref=ref, send_sem=ag_ss.at[d], recv_sem=ag_rs.at[d],
+            device_id={FS: to}, device_id_type=pl.DeviceIdType.MESH)
+
+    def lows():
+        for dz, dy in plane_far_first:
+            ag_copy(dz, dy, back=True).wait_recv()
+
     others = sums.at[pl.ds(0, N_FS * N_TP - 1)]
 
     def reduce_partials():
@@ -338,84 +334,91 @@
             pltpu.make_async_remote_copy(
                 src_ref=sums.at[me], dst_ref=sums.at[me], send_sem=sum_ss, recv_sem=sum_rs,
                 device_id={FS: zs[dz] * SIDE + ys[dy], TP: ts[dt]}, device_id_type=pl.DeviceIdType.MESH).start()
-        lax.fori_loop(1, N_FS, start(ag_copy), 0)
+        for dz, dy in plane_far_first:
+            ag_copy(dz, dy).start()
 
     def clip():
         pltpu.make_async_copy(others, others, sum_rs).wait()
         scale[...] = jnp.broadcast_to(
             jnp.minimum(1.0, target / jnp.sqrt(jnp.sum(sums[...], axis=0))), scale.shape)
 
-    def from_a(m):
-        for g, pg in enumerate(pgs):
-            to_sib(g, pg.take_a(m) if m < 3 else pg.take_a2())
-
-    def from_b(m):
-        for g, pg in enumerate(pgs):
-            to_sib(g, *pg.take_b(m))
-
-    def from_b2(m):
-        for g, pg in enumerate(pgs):
-            to_sib(g, pg.take_b2(m))
-
-    steps = dict(a=from_a, b=from_b, c=from_b2, w=w_stage, t=transposes, g=gradient_o, q=gradient_q, near=project_near, far=project_far,
+    along_a = [a, a1, a2, a3]
+    steps = dict(a=lambda m: to_x(pg.take_a(m) if m < 3 else pg.take_a2()), b=lambda m: to_x(*pg.take_b(m)),
+                 c=lambda m: to_x(pg.take_b2(m)), xa=lambda m: from_x(fs_of(along_a[m], b)),
+                 xb=lambda m: from_x(fs_of(along_a[m], b1), fs_of(along_a[m], b2)),
+                 xc=lambda m: from_x(fs_of(along_a[m], b3)), w=w_stage, t=transposes, g=gradient_o, q=gradient_q, near=project_near, far=project_far,
                  send=send_partials, reduce=reduce_partials, clip=clip,
-                 lows=lambda: arrivals(lowg, i, N_FS, FS, ag_rs))
+                 lows=lows)
     for name, *args in ORDER:
         steps[name](*args)
     pltpu.make_async_copy(others, others, sum_ss).wait()
-    for g in pgs + wgs:
+    for g in [pg] + wgs:
         g.finish()
-    for cp in sib_sent:
+    for cp in sent:
         cp.wait_send()
-    lax.fori_loop(1, N_FS, wait_send(rs_copy), 0)
-    lax.fori_loop(1, N_FS, wait_send(ag_copy), 0)
-
-
-def update_kernel(pf, pw, lowg, low, scale, pq, po, wq, wo, fq, sq, fo, so,
-                  nwq, nwo, nfq, nsq, nfo, nso, stq, sto, cpq, cpo, dirs):
+    for dz, dy in plane_far_first:
+        rs_copy(dz, dy).wait_send()
+    for dz, dy in plane_far_first:
+        ag_copy(dz, dy).wait_send()
+
+
+def update_kernel(pf, pw, lowg, low, scale, pq, po, wq, wo, fq, sq, fo, so, *refs):
+    held, (dirs, *bufs, sems) = refs[:10], refs[10:]
+    nwq, nwo, nfq, nsq, nfo, nso, stq, sto, cpq, cpo = bufs
     cq, co = fq.shape[1], fo.shape[1]
     nq, no, rows = pq.shape[0], po.shape[0], fq.shape[0]
-    g = pl.program_id(0)
-    n = cpq.shape[0] // nq
+    n = N_FS // CHUNKS
     blocks = (cq + co) // 128
     at_o = (cq // 128) * nq
     at_f = at_o + (co // 128) * no
     s = scale[0:1, 0:1]
-
-    @pl.when(g == 0)
-    def _():
-        for j in range(blocks):
-            f = pw[:, at_f + j * rows:at_f + (j + 1) * rows, :].astype(F32)
-            v = pw[:, at_f + (blocks + j) * rows:at_f + (blocks + j + 1) * rows, :].astype(F32)
-            l = lowg[:, :, j * 128:(j + 1) * 128].astype(F32)
-            d = moments(f, v, l, s)[2]
-            dirs[:, j * 128:(j + 1) * 128] = (-step_rate * d).reshape(-1, 128).astype(BF16)
-
+    outgoing = []
+
+    def write(k, part=None):
+        src, dst = bufs[k], held[k]
+        if part is not None:
+            src, dst = src.at[part], dst.at[part]
+        cp = pltpu.make_async_copy(src, dst, sems.at[len(outgoing)])
+        cp.start()
+        outgoing.append(cp)
+
+    for j in range(blocks):
+        f = pw[:, at_f + j * rows:at_f + (j + 1) * rows, :].astype(F32)
+        v = pw[:, at_f + (blocks + j) * rows:at_f + (blocks + j + 1) * rows, :].astype(F32)
+        l = lowg[:, :, j * 128:(j + 1) * 128].astype(F32)
+        d = moments(f, v, l, s)[2]
+        dirs[:, j * 128:(j + 1) * 128] = (-step_rate * d).reshape(-1, 128).astype(BF16)
     dq, do = dirs[:, :cq], dirs[:, cq:]
-    own = pl.ds(g * n, n)
-    whole = pf[own].reshape(n, nq + no, pf.shape[3])
-    mq = dot(whole[:, :nq, :].reshape(n * nq, -1), dq)
-    mo = dot(whole[:, nq:, :].reshape(n * no, -1), do)
-    for col in range(0, cq, 128):
-        w = pw[own, (col // 128) * nq:(col // 128 + 1) * nq, :].astype(F32).reshape(n * nq, 128)
-        cpq[:, col:col + 128] = (w + mq[:, col:col + 128]).astype(BF16)
-    for col in range(0, co, 128):
-        at = at_o + (col // 128) * no
-        w = pw[own, at:at + no, :].astype(F32).reshape(n * no, 128)
-        cpo[:, col:col + 128] = (w + mo[:, col:col + 128]).astype(BF16)
-
-    @pl.when(g == 0)
-    def _():
-        f, v, _ = moments(fq[...], sq[...], low[:, :cq], s)
-        nfq[...] = f
-        nsq[...] = v
-        f, v, _ = moments(fo[...], so[...], low[:, cq:], s)
-        nfo[...] = f
-        nso[...] = v
-        for p_, d_, w_, st_, nw_ in ((pq, dq, wq, stq, nwq), (po, do, wo, sto, nwo)):
-            step = dot(p_[...], d_) * (-1.0 / step_rate) + decay_rate * w_[...]
-            st_[...] = step
-            nw_[...] = w_[...] - step_rate * step
+
+    for g in range(CHUNKS):
+        own = slice(g * n, (g + 1) * n)
+        whole = pf[own].reshape(n, nq + no, pf.shape[3])
+        mo = dot(whole[:, nq:, :].reshape(n * no, -1), do)
+        at = pl.ds(g * n * no, n * no)
+        for col in range(0, co, 128):
+            lo = at_o + (col // 128) * no
+            w = pw[own, lo:lo + no, :].astype(F32).reshape(n * no, 128)
+            cpo[at, col:col + 128] = (w + mo[:, col:col + 128]).astype(BF16)
+        write(9, at)
+        mq = dot(whole[:, :nq, :].reshape(n * nq, -1), dq)
+        at = pl.ds(g * n * nq, n * nq)
+        for col in range(0, cq, 128):
+            w = pw[own, (col // 128) * nq:(col // 128 + 1) * nq, :].astype(F32).reshape(n * nq, 128)
+            cpq[at, col:col + 128] = (w + mq[:, col:col + 128]).astype(BF16)
+        write(8, at)
+        if g == 0:
+            for p_, d_, w_, st_, nw_ in ((pq, dq, wq, stq, nwq), (po, do, wo, sto, nwo)):
+                step = dot(p_[...], d_) * (-1.0 / step_rate) + decay_rate * w_[...]
+                st_[...] = step
+                nw_[...] = w_[...] - step_rate * step
+            for k in (6, 7, 0, 1):
+                write(k)
+            nfq[...], nsq[...], _ = moments(fq[...], sq[...], low[:, :cq], s)
+            nfo[...], nso[...], _ = moments(fo[...], so[...], low[:, cq:], s)
+            for k in (2, 3, 4, 5):
+                write(k)
+    for cp in outgoing:
+        cp.wait()
 
 
 def per_device(query_latent_rows, grad_q, head_out, grad_out, proj_q, proj_o, query_up_weight, weight_o,
@@ -449,8 +452,8 @@
             V((co, tokens), BF16), V((cq, tokens), BF16), V((co, N_FS * no), BF16), V((cq, N_FS * nq), BF16),
             V((co, rank), F32), V((cq, rank), F32), V((N_FS, rows, cq + co), BF16), V((N_FS, rows, cq + co), BF16),
             V((N_FS * N_TP, 1, 128), F32),
-            dma((16,)), dma((NP, 20)), dma((NP, 20)), dma((NW, 20)), dma((NW, 20)),
-            dma((NP, N_FS)), dma((NP, N_FS)),
+            dma((16,)), dma((20,)), dma((20,)), dma((NW, 20)), dma((NW, 20)),
+            dma((N_FS,)), dma((N_FS,)), dma((2, N_FS)), dma((2, N_FS)),
             dma((N_FS,)), dma, dma, dma, dma((N_FS,)), dma((N_FS,)),
         ],
         compiler_params=pltpu.CompilerParams(collective_id=0, has_side_effects=True,
@@ -458,20 +461,16 @@
         name="exchange",
     )(*[pltpu.with_memory_space_constraint(x, pltpu.HBM) for x in ins])
 
-    G = 2
-    n = N_FS // G
-    full = lambda x: pl.BlockSpec(x.shape, lambda g: (0,) * len(x.shape))
     outs = [sds((nq, cq), F32), sds((no, co), F32), sds((rows, cq), F32), sds((rows, cq), F32),
-            sds((rows, co), F32), sds((rows, co), F32), sds((nq, cq), F32), sds((no, co), F32)]
+            sds((rows, co), F32), sds((rows, co), F32), sds((nq, cq), F32), sds((no, co), F32),
+            sds((N_FS * nq, cq), BF16), sds((N_FS * no, co), BF16)]
     ops = (*gathered, proj_q, proj_o, query_up_weight, weight_o, first_q, second_q, first_o, second_o)
     return tuple(pl.pallas_call(
         update_kernel,
-        grid=(G,),
-        in_specs=[full(x) for x in ops],
-        out_specs=[full(o) for o in outs] + [pl.BlockSpec((n * nq, cq), lambda g: (g, 0)),
-                                             pl.BlockSpec((n * no, co), lambda g: (g, 0))],
-        out_shape=outs + [sds((N_FS * nq, cq), BF16), sds((N_FS * no, co), BF16)],
-        scratch_shapes=[V((rows * N_FS, cq + co), BF16)],
+        in_specs=[pl.BlockSpec(memory_space=pltpu.VMEM)] * len(ops),
+        out_specs=[pl.BlockSpec(memory_space=pltpu.HBM)] * len(outs),
+        out_shape=outs,
+        scratch_shapes=[V((rows * N_FS, cq + co), BF16)] + [like(o) for o in outs] + [dma((8 + 2 * CHUNKS,))],
         compiler_params=pltpu.CompilerParams(vmem_limit_bytes=24 * 1024 * 1024),
         name="update",
     )(*ops))

time: 50.6 us -> 49.3 us (0.974)
  Pallas kernels: 49.7 us -> 48.4 us
    pallas_call x1, Pallas kernels: 46.3 us -> 45.5 us  [per_device(): pl.pallas_call(ex, out_shape=[V((N_FS, 2, half, rank), BF16), V((N_FS, wr...]
where the time goes in v4:
time: 49.3 us; the launch traced here: 49.2 us
  Pallas kernels  48.4 us (98%)
  between operations  0.78 us (2%)
    pallas_call x1, Pallas kernels, per_device(): pl.pallas_call(ex, out_shape=[V((N_FS, 2, half, rank), BF16), V((N_FS, wr...  45.5 us
    pallas_call x1, Pallas kernels, per_device(): pl.pallas_call(update_kernel, in_specs=[pl.BlockSpec(memory_space=pltpu.V...  2.92 us

profile of v4, /device:TPU:1, one launch (start us, length us, event | category | flops | bytes accessed | tf_op | source)
XLA Modules:
  0.0 49.2 jit_solution(17475588726273369412)
XLA Ops:
  0.6 0.0 copy-start.7
  0.7 0.0 copy-start.6
  0.7 0.0 copy-start.5
  0.7 0.0 copy-start.4
  0.7 0.0 copy-start
  0.7 0.0 copy-start.2
  0.7 0.0 copy-start.1
  0.7 0.0 copy-start.3
  0.7 45.5 %exchange.1 = (bf16[16,2,160,256]{3,2,1,0:T(8,128)(2,1)S(1)}, bf16[16,864,128]{2,1,0:T(8,128)(2,1)S(1)}, bf16[16,16,640]{2,1,0:T(8,128)(2,1)S(1)}, f32[16,640]{1,0:T(8,128)S(1)}, f32[8,128]{1,0:T(8,128)S(1)}) custom-call(bf16[1536,1024]{1,0:T(8,128)(2,1)} %refs_0_.1, bf16[1536,384]{1,0:T(8,128)(2,1)} %refs_1_.1, bf16[1536,256]{1,0:T(8,128)(2,1)} %refs_2_.1, ...), custom_call_target="tpu_custom_call" | custom-call | tf_op jit(solution)/shard_map/exchange/pallas_call | solution.py:443
  46.2 0.0 copy-done.7
  46.2 0.0 copy-done.6
  46.2 0.0 copy-done.5
  46.2 0.0 copy-done.4
  46.2 0.0 copy-done
  46.3 0.0 copy-done.2
  46.3 0.0 copy-done.1
  46.3 0.0 copy-done.3
  46.3 2.9 %update.1 = (f32[64,384]{1,0:T(8,128)}, f32[256,256]{1,0:T(8,128)}, f32[16,384]{1,0:T(8,128)}, f32[16,384]{1,0:T(8,128)}, f32[16,256]{1,0:T(8,128)}, /*index=5*/...) custom-call(bf16[16,2,160,256]{3,2,1,0:T(8,128)(2,1)S(1)} %get-tuple, ...), custom_call_target="tpu_custom_call" | custom-call | tf_op jit(solution)/shard_map/update/pallas_call | solution.py:468
Async XLA Ops:
  0.6 45.6 %copy-start.7 = (f32[16,256]{1,0:T(8,128)S(1)}, f32[16,256]{1,0:T(8,128)}, u32[]{:S(2)}) copy-start(f32[16,256]{1,0:T(8,128)} %so.1) | copy-start | bytes 49156
  0.7 45.6 %copy-start.6 = (f32[16,256]{1,0:T(8,128)S(1)}, f32[16,256]{1,0:T(8,128)}, u32[]{:S(2)}) copy-start(f32[16,256]{1,0:T(8,128)} %fo.1) | copy-start | bytes 49156
  0.7 45.6 %copy-start.5 = (f32[16,384]{1,0:T(8,128)S(1)}, f32[16,384]{1,0:T(8,128)}, u32[]{:S(2)}) copy-start(f32[16,384]{1,0:T(8,128)} %sq.1) | copy-start | bytes 73732
  0.7 45.6 %copy-start.4 = (f32[16,384]{1,0:T(8,128)S(1)}, f32[16,384]{1,0:T(8,128)}, u32[]{:S(2)}) copy-start(f32[16,384]{1,0:T(8,128)} %fq.1) | copy-start | bytes 73732
  0.7 45.6 %copy-start = (f32[256,256]{1,0:T(8,128)S(1)}, f32[256,256]{1,0:T(8,128)}, u32[]{:S(2)}) copy-start(f32[256,256]{1,0:T(8,128)} %wo.1) | copy-start | bytes 786436
  0.7 45.6 %copy-start.2 = (f32[64,384]{1,0:T(8,128)S(1)}, f32[64,384]{1,0:T(8,128)}, u32[]{:S(2)}) copy-start(f32[64,384]{1,0:T(8,128)} %wq.1) | copy-start | bytes 294916
  0.7 45.6 %copy-start.1 = (bf16[256,256]{1,0:T(8,128)(2,1)S(1)}, bf16[256,256]{1,0:T(8,128)(2,1)}, u32[]{:S(2)}) copy-start(bf16[256,256]{1,0:T(8,128)(2,1)} %po.1) | copy-start | bytes 393220
  0.7 45.6 %copy-start.3 = (bf16[64,256]{1,0:T(8,128)(2,1)S(1)}, bf16[64,256]{1,0:T(8,128)(2,1)}, u32[]{:S(2)}) copy-start(bf16[64,256]{1,0:T(8,128)(2,1)} %pq.1) | copy-start | bytes 98308

commit v5 on v4

--- a/solution.py
+++ b/solution.py
@@ -21,7 +21,16 @@
 
 CHUNKS = 4
 NW = 1
-ORDER = [('w', 0, 0), ('t',), ('g', 0), ('g', 1), ('g', 2), ('a', 1), ('a', 2), ('b', 0), ('g', 3), ('a', 3), ('g', 4), ('g', 5), ('xa', 1), ('xa', 2), ('xb', 0), ('b', 1), ('b', 2), ('g', 6), ('g', 7), ('b', 3), ('w', 0, 1), ('xa', 3), ('c', 0), ('g', 8), ('g', 9), ('xb', 1), ('xb', 2), ('c', 1), ('c', 2), ('g', 10), ('g', 11), ('xb', 3), ('c', 3), ('xc', 0), ('w', 0, 2), ('g', 12), ('g', 13), ('g', 14), ('g', 15), ('q', 0), ('q', 1), ('xc', 1), ('xc', 2), ('q', 2), ('q', 3), ('xc', 3), ('near',), ('far',), ('w', 0, 3), ('send',), ('w', 0, 4), ('reduce',), ('w', 0, 5), ('clip',), ('lows',)]
+ORDER = [
+    ("w", 0, 0), ("t",), ("g", 0), ("g", 1), ("g", 2), ("a", 1), ("a", 2),
+    ("b", 0), ("g", 3), ("a", 3), ("g", 4), ("g", 5), ("xa", 1), ("xa", 2),
+    ("xb", 0), ("b", 1), ("b", 2), ("g", 6), ("g", 7), ("b", 3), ("w", 0, 1),
+    ("xa", 3), ("c", 0), ("g", 8), ("g", 9), ("xb", 1), ("xb", 2), ("c", 1),
+    ("c", 2), ("g", 10), ("g", 11), ("xb", 3), ("c", 3), ("w", 0, 2), ("xc", 0),
+    ("g", 12), ("g", 13), ("g", 14), ("g", 15), ("q", 0), ("q", 1), ("xc", 1),
+    ("xc", 2), ("q", 2), ("q", 3), ("xc", 3), ("near",), ("far",), ("send",),
+    ("w", 0, 3), ("w", 0, 4), ("reduce",), ("clip",), ("w", 0, 5), ("lows",),
+]
 
 
 def dot(a, b):

time: 49.3 us -> 47.7 us (0.968)
  Pallas kernels: 48.4 us -> 46.8 us
    pallas_call x1, Pallas kernels: 45.5 us -> 43.9 us  [per_device(): pl.pallas_call(ex, out_shape=[V((N_FS, 2, half, rank), BF16), V((N_FS, wr...]
where the time goes in v5:
time: 47.7 us; the launch traced here: 47.6 us
  Pallas kernels  46.8 us (98%)
  between operations  0.78 us (2%)
    pallas_call x1, Pallas kernels, per_device(): pl.pallas_call(ex, out_shape=[V((N_FS, 2, half, rank), BF16), V((N_FS, wr...  43.9 us
    pallas_call x1, Pallas kernels, per_device(): pl.pallas_call(update_kernel, in_specs=[pl.BlockSpec(memory_space=pltpu.V...  2.92 us

profile of v5, /device:TPU:1, one launch (start us, length us, event | category | flops | bytes accessed | tf_op | source)
XLA Modules:
  0.0 47.6 jit_solution(550154511863936045)
XLA Ops:
  0.6 0.0 copy-start.7
  0.7 0.0 copy-start.6
  0.7 0.0 copy-start.5
  0.7 0.0 copy-start.4
  0.7 0.0 copy-start
  0.7 0.0 copy-start.2
  0.7 0.0 copy-start.1
  0.7 0.0 copy-start.3
  0.7 43.9 %exchange.1 = (bf16[16,2,160,256]{3,2,1,0:T(8,128)(2,1)S(1)}, bf16[16,864,128]{2,1,0:T(8,128)(2,1)S(1)}, bf16[16,16,640]{2,1,0:T(8,128)(2,1)S(1)}, f32[16,640]{1,0:T(8,128)S(1)}, f32[8,128]{1,0:T(8,128)S(1)}) custom-call(bf16[1536,1024]{1,0:T(8,128)(2,1)} %refs_0_.1, bf16[1536,384]{1,0:T(8,128)(2,1)} %refs_1_.1, bf16[1536,256]{1,0:T(8,128)(2,1)} %refs_2_.1, ...), custom_call_target="tpu_custom_call" | custom-call | tf_op jit(solution)/shard_map/exchange/pallas_call | solution.py:452
  44.6 0.0 copy-done.7
  44.6 0.0 copy-done.6
  44.6 0.0 copy-done.5
  44.6 0.0 copy-done.4
  44.6 0.0 copy-done
  44.7 0.0 copy-done.2
  44.7 0.0 copy-done.1
  44.7 0.0 copy-done.3
  44.7 2.9 %update.1 = (f32[64,384]{1,0:T(8,128)}, f32[256,256]{1,0:T(8,128)}, f32[16,384]{1,0:T(8,128)}, f32[16,384]{1,0:T(8,128)}, f32[16,256]{1,0:T(8,128)}, /*index=5*/...) custom-call(bf16[16,2,160,256]{3,2,1,0:T(8,128)(2,1)S(1)} %get-tuple, ...), custom_call_target="tpu_custom_call" | custom-call | tf_op jit(solution)/shard_map/update/pallas_call | solution.py:477
Async XLA Ops:
  0.6 44.0 %copy-start.7 = (f32[16,256]{1,0:T(8,128)S(1)}, f32[16,256]{1,0:T(8,128)}, u32[]{:S(2)}) copy-start(f32[16,256]{1,0:T(8,128)} %so.1) | copy-start | bytes 49156
  0.7 44.0 %copy-start.6 = (f32[16,256]{1,0:T(8,128)S(1)}, f32[16,256]{1,0:T(8,128)}, u32[]{:S(2)}) copy-start(f32[16,256]{1,0:T(8,128)} %fo.1) | copy-start | bytes 49156
  0.7 44.0 %copy-start.5 = (f32[16,384]{1,0:T(8,128)S(1)}, f32[16,384]{1,0:T(8,128)}, u32[]{:S(2)}) copy-start(f32[16,384]{1,0:T(8,128)} %sq.1) | copy-start | bytes 73732
  0.7 44.0 %copy-start.4 = (f32[16,384]{1,0:T(8,128)S(1)}, f32[16,384]{1,0:T(8,128)}, u32[]{:S(2)}) copy-start(f32[16,384]{1,0:T(8,128)} %fq.1) | copy-start | bytes 73732
  0.7 44.0 %copy-start = (f32[256,256]{1,0:T(8,128)S(1)}, f32[256,256]{1,0:T(8,128)}, u32[]{:S(2)}) copy-start(f32[256,256]{1,0:T(8,128)} %wo.1) | copy-start | bytes 786436
  0.7 44.0 %copy-start.2 = (f32[64,384]{1,0:T(8,128)S(1)}, f32[64,384]{1,0:T(8,128)}, u32[]{:S(2)}) copy-start(f32[64,384]{1,0:T(8,128)} %wq.1) | copy-start | bytes 294916
  0.7 44.0 %copy-start.1 = (bf16[256,256]{1,0:T(8,128)(2,1)S(1)}, bf16[256,256]{1,0:T(8,128)(2,1)}, u32[]{:S(2)}) copy-start(bf16[256,256]{1,0:T(8,128)(2,1)} %po.1) | copy-start | bytes 393220
  0.7 44.0 %copy-start.3 = (bf16[64,256]{1,0:T(8,128)(2,1)S(1)}, bf16[64,256]{1,0:T(8,128)(2,1)}, u32[]{:S(2)}) copy-start(bf16[64,256]{1,0:T(8,128)(2,1)} %pq.1) | copy-start | bytes 98308
